TPU v7x, 32 devices: a whole 2x2x4 slice. The times are simulated.
32 devices in a mesh: sp: 4 (over y, x), dp: 8 (over z, core).
Axes of the slice: x: 2, y: 2, z: 4, core: 2. Of those that a mesh axis runs over, the one named last changes fastest.
Arguments:
- tokens: bfloat16 [8, 1024, 2048], P('dp', 'sp'), may hold values from -200 to 200
- w_qdown: bfloat16 [2048, 512], P('dp'), may hold values from -0.125 to 0.125
- w_kvdown: bfloat16 [2048, 512], P('dp'), may hold values from -0.125 to 0.125
- w_rotary: bfloat16 [2048, 64], replicated, may hold values from -0.125 to 0.125
- q_gain: float32 [512], replicated, may hold values from 0.1 to 1.9
- kv_gain: float32 [512], replicated, may hold values from 0.1 to 1.9
- w_qup: bfloat16 [512, 3072], P('dp'), may hold values from -1 to 1
- w_kvup: bfloat16 [512, 4096], P('dp'), may hold values from -1 to 1
- w_out: bfloat16 [2048, 2048], P(None, 'dp'), may hold values from -0.125 to 0.125
- out_gain: float32 [2048], replicated, may hold values from 0.1 to 1.9
Outputs:
- mixed: bfloat16 [8, 1024, 2048], P('dp', 'sp')
All inputs are finite; a program needn't handle non-finite values.
Results may differ from a plain program's by a relative error of at most 0.01.
The roundings to bfloat16 on the way count: a program that leaves them out, or rounds other values in their place, can miss the bound.
Values may be sent and summed in bfloat16 or wider, within the bound.
A program may use at most 128 MiB of HBM per device.

v0:
```python
import functools
import math

import jax
import jax.numpy as jnp
import numpy as np
from jax import lax
from jax.experimental import pallas as pl
from jax.experimental.pallas import tpu as pltpu
from jax.sharding import PartitionSpec as P

HEADS = 16
NOPE = 128
ROPE = 64
VDIM = 128


EPSILON = 1e-06
THETA = 10000.0
LANES = 128
SUBLANES = 16
MESH = pl.DeviceIdType.MESH


def norm_rows(values, gain):
    scale = lax.rsqrt(jnp.mean(values * values, axis=-1, keepdims=True) + EPSILON)
    return values * scale * gain


def rotate(values, cosine, sine):
    half = values.shape[-1] // 2
    first = values[..., :half]
    second = values[..., half:]
    return jnp.concatenate(
        [first * cosine - second * sine, second * cosine + first * sine], axis=-1
    )


def turn_tables(offset, count):
    positions = (offset + jnp.arange(count)).astype(jnp.float32)
    freqs = THETA ** (-jnp.arange(0, ROPE, 2).astype(jnp.float32) / ROPE)
    angles = positions[:, None] * freqs[None, :]
    return (jnp.cos(angles), jnp.sin(angles))


def make_queries(q_full, cosine, sine, heads_here):
    rows = q_full.shape[0]
    shaped = q_full.reshape(rows, heads_here, NOPE + ROPE)
    turned = rotate(shaped[..., NOPE:], cosine[:, None, :], sine[:, None, :])
    joined = jnp.concatenate([shaped[..., :NOPE], turned], axis=-1)
    return joined.reshape(rows, heads_here * (NOPE + ROPE)).astype(jnp.bfloat16)


def attend(query_heads, keyval_heads, key_rot, heads_here):
    length = query_heads.shape[0]
    block = math.gcd(length, 512)
    scaling = (NOPE + ROPE) ** (-0.5)
    queries = query_heads.reshape(length, heads_here, NOPE + ROPE)
    keyval = keyval_heads.reshape(length, heads_here, NOPE + VDIM)
    keys_all = keyval[..., :NOPE]
    values_all = keyval[..., NOPE:]
    outputs = []
    for begin in range(0, length, block):
        finish = begin + block
        query_block = queries[begin:finish]
        scores = jnp.einsum(
            "qhd,khd->hqk",
            query_block[..., :NOPE],
            keys_all[:finish],
            preferred_element_type=jnp.float32,
        )
        scores = scores + jnp.einsum(
            "qhd,kd->hqk",
            query_block[..., NOPE:],
            key_rot[:finish],
            preferred_element_type=jnp.float32,
        )
        scores = scores * scaling
        query_pos = begin + jnp.arange(block)
        key_pos = jnp.arange(finish)
        allowed = key_pos[None, :] <= query_pos[:, None]
        scores = jnp.where(allowed[None], scores, -jnp.inf)
        top = jnp.max(scores, axis=-1, keepdims=True)
        expo = jnp.exp(scores - top)
        weights = (expo / jnp.sum(expo, axis=-1, keepdims=True)).astype(jnp.bfloat16)
        attended = jnp.einsum(
            "hqk,khd->qhd", weights, values_all[:finish], preferred_element_type=jnp.float32
        )
        outputs.append(attended.astype(jnp.bfloat16))
    return jnp.concatenate(outputs, axis=0).reshape(length, heads_here * VDIM)


def plain_body(tokens, w_qdown, w_kvdown, w_rotary, q_gain, kv_gain, w_qup, w_kvup, w_out, out_gain):
    own_rows = tokens[0]
    tok_count = own_rows.shape[0]
    sp_count = lax.axis_size("sp")
    sp_place = lax.axis_index("sp")
    length = tok_count * sp_count
    heads_here = HEADS // sp_count
    pieces = (
        lax.all_gather(w_qdown, "dp", axis=0, tiled=True),
        lax.all_gather(w_kvdown, "dp", axis=0, tiled=True),
    )
    q_lat = jnp.dot(own_rows, pieces[0], preferred_element_type=jnp.float32)
    kv_lat = jnp.dot(own_rows, pieces[1], preferred_element_type=jnp.float32)
    q_norm = norm_rows(q_lat, q_gain).astype(jnp.bfloat16)
    kv_norm = norm_rows(kv_lat, kv_gain).astype(jnp.bfloat16)
    own_cos, own_sin = turn_tables(sp_place * tok_count, tok_count)
    key_rot = rotate(
        jnp.dot(own_rows, w_rotary, preferred_element_type=jnp.float32), own_cos, own_sin
    ).astype(jnp.bfloat16)
    q_all, kv_all, rot_all = (
        lax.all_gather(q_norm, "sp", axis=0, tiled=True),
        lax.all_gather(kv_norm, "sp", axis=0, tiled=True),
        lax.all_gather(key_rot, "sp", axis=0, tiled=True),
    )
    q_width = heads_here * (NOPE + ROPE)
    kv_width = heads_here * (NOPE + VDIM)
    q_columns = lax.dynamic_slice_in_dim(w_qup, sp_place * q_width, q_width, 1)
    kv_columns = lax.dynamic_slice_in_dim(w_kvup, sp_place * kv_width, kv_width, 1)
    pieces = (
        lax.all_gather(q_columns, "dp", axis=0, tiled=True),
        lax.all_gather(kv_columns, "dp", axis=0, tiled=True),
    )
    q_full = jnp.dot(q_all, pieces[0], preferred_element_type=jnp.float32)
    kv_full = jnp.dot(kv_all, pieces[1], preferred_element_type=jnp.float32)
    all_cos, all_sin = turn_tables(0, length)
    query_heads = make_queries(q_full, all_cos, all_sin, heads_here)
    keyval_heads = kv_full.astype(jnp.bfloat16)
    attended = attend(query_heads, keyval_heads, rot_all, heads_here)
    merged = lax.all_to_all(attended, "sp", split_axis=0, concat_axis=1, tiled=True)
    proj = jnp.dot(
        merged, lax.all_gather(w_out, "dp", axis=1, tiled=True), preferred_element_type=jnp.float32
    )
    mixed = norm_rows(proj, out_gain).astype(jnp.bfloat16)
    return mixed[None]


def turn_table(length):
    positions = np.arange(length, dtype=np.float32)
    freqs = np.float32(THETA) ** (-np.arange(0, ROPE, 2).astype(np.float32) / np.float32(ROPE))
    angles = positions[:, None] * freqs[None, :].astype(np.float32)
    cosine, sine = np.cos(angles), np.sin(angles)
    return np.concatenate([cosine, cosine, sine, sine], axis=1).astype(np.float32)


class Copies:
    def __init__(self, send_sems, recv_sems):
        self.send_sems, self.recv_sems = send_sems, recv_sems
        self.used = 0
        self.sent = []

    def start(self, source, target, device):
        at = self.used
        self.used += 1
        copy = pltpu.make_async_remote_copy(
            src_ref=source,
            dst_ref=target,
            send_sem=self.send_sems.at[at],
            recv_sem=self.recv_sems.at[at],
            device_id=device,
            device_id_type=MESH,
        )
        copy.start()
        self.sent.append(copy)
        return copy


class PlaneSpread:
    def __init__(self, copies, place, view, rows):
        self.copies, self.place, self.view, self.rows = copies, place, view, rows

    def send(self):
        me, rows = self.place["me"], self.rows
        block = self.view(me, 0, rows)
        self.along_x = self.copies.start(block, block, {"sp": self.place["x"]})
        self.along_y = self.copies.start(block, block, {"sp": self.place["y"]})

    def relay(self):
        half = self.rows // 2
        self.along_x.wait_recv()
        block = self.view(self.place["x"], 0, half)
        self.first = self.copies.start(block, block, {"sp": self.place["y"]})
        self.along_y.wait_recv()
        block = self.view(self.place["y"], half, half)
        self.second = self.copies.start(block, block, {"sp": self.place["x"]})

    def finish(self):
        self.first.wait_recv()
        self.second.wait_recv()


class WeightGather:
    def __init__(self, copies, place, source, buffer, local_sem, tail=0):
        self.copies, self.place, self.source, self.buffer = copies, place, source, buffer
        self.rows = (source.shape[0] - tail) // place["sp_count"]
        self.tail = pl.ds(source.shape[0] - tail, tail)
        self.local_sem = local_sem
        self.steps = range(1, place["z_count"])
        self.planes = {}

    def piece(self, slot, owner, begin, count):
        start = pl.multiple_of(owner * self.rows + begin, SUBLANES)
        return self.buffer.at[slot, pl.ds(start, count), :]

    def start(self):
        place, rows = self.place, self.rows
        own = self.source.at[pl.ds(pl.multiple_of(place["me"] * rows, SUBLANES), rows), :]
        self.arrivals = {}
        for step in self.steps:
            target = self.piece(place["dp"], place["me"], 0, rows)
            device = {"dp": lax.rem(place["dp"] + 2 * step, place["dp_count"])}
            self.arrivals[step] = self.copies.start(own, target, device)

    def start_tail(self):
        place = self.place
        own = self.source.at[self.tail, :]
        target = self.buffer.at[place["dp"], self.tail, :]
        self.tails = {}
        for step in self.steps:
            device = {"dp": lax.rem(place["dp"] + 2 * step, place["dp_count"])}
            self.tails[step] = self.copies.start(own, target, device)

    def cross_tail(self, step):
        self.tails[step].wait_recv()
        block = self.buffer.at[self.slot(step), self.tail, :]
        self.crossed.append(self.copies.start(block, block, {"dp": self.place["core"]}))

    def keep(self):
        place = self.place
        self.crossed = [
            self.copies.start(self.source, self.buffer.at[place["dp"]], {"dp": place["core"]})
        ]
        self.local = None
        if self.local_sem is None:
            self.buffer[place["dp"]] = self.source[...]
        else:
            self.local = pltpu.make_async_copy(
                self.source, self.buffer.at[place["dp"]], self.local_sem
            )
            self.local.start()

    def slot(self, step):
        place = self.place
        return lax.rem(place["dp"] + place["dp_count"] - 2 * step, place["dp_count"])

    def cross(self, step, owner):
        block = self.piece(self.slot(step), owner, 0, self.rows)
        self.crossed.append(self.copies.start(block, block, {"dp": self.place["core"]}))

    def spread(self, step):
        self.arrivals[step].wait_recv()
        view = functools.partial(self.piece, self.slot(step))
        plane = PlaneSpread(self.copies, self.place, view, self.rows)
        plane.send()
        self.planes[step] = plane
        self.cross(step, self.place["me"])

    def relay(self, step):
        self.planes[step].relay()
        self.cross(step, self.place["x"])
        self.cross(step, self.place["y"])

    def close(self, step):
        self.planes[step].finish()
        self.cross(step, self.place["far"])

    def finish(self):
        if self.local is not None:
            self.local.wait()
        for copy in self.crossed:
            copy.wait_recv()


class ColumnGather:
    def __init__(self, copies, place, source, buffer, local_sem):
        self.copies, self.place, self.source, self.buffer = copies, place, source, buffer
        self.local_sem = local_sem
        width = buffer.shape[2]
        self.columns = pl.ds(pl.multiple_of(place["me"] * width, LANES), width)

    def start(self):
        place = self.place
        own = self.source.at[:, self.columns]
        target = self.buffer.at[place["dp"]]
        self.arrivals = []
        for step in range(1, place["z_count"]):
            device = {"dp": lax.rem(place["dp"] + 2 * step, place["dp_count"])}
            self.arrivals.append(self.copies.start(own, target, device))

    def keep(self):
        place = self.place
        own = self.source.at[:, self.columns]
        target = self.buffer.at[place["dp"]]
        self.crossed = [self.copies.start(own, target, {"dp": place["core"]})]
        self.local = pltpu.make_async_copy(own, target, self.local_sem)
        self.local.start()

    def cross(self):
        place = self.place
        for step in range(1, place["z_count"]):
            self.arrivals[step - 1].wait_recv()
            slot = lax.rem(place["dp"] + place["dp_count"] - 2 * step, place["dp_count"])
            block = self.buffer.at[slot]
            self.crossed.append(self.copies.start(block, block, {"dp": place["core"]}))

    def finish(self):
        self.local.wait()
        for copy in self.crossed:
            copy.wait_recv()


def rotary_picks(rows, offset, skip):
    width = skip + 2 * ROPE
    row = lax.broadcasted_iota(jnp.int32, (rows, width), 0)
    col = lax.broadcasted_iota(jnp.int32, (rows, width), 1)
    half = ROPE // 2
    minus = (col >= skip + ROPE) & (col < skip + ROPE + half)
    origin = jnp.where(
        col < skip + ROPE, col, jnp.where(minus, col - half, col - ROPE - half)
    )
    sign = jnp.where(minus, -1.0, 1.0)
    return jnp.where(row == origin + offset, sign, 0.0).astype(jnp.bfloat16)


def turned(values, table):
    product = values * table
    return product + pltpu.roll(product, ROPE, axis=1)


def dot(left, right):
    return jnp.dot(left, right, preferred_element_type=jnp.float32)


def kernel(
    sp_count, dp_count,
    tokens, w_qdown, w_kvdown, w_rotary, q_gain, kv_gain, w_qup, w_kvup, w_out, out_gain, table,
    out,
    qd_all, kvd_all, qu_all, kvu_all, wo_all, q_lat, kv_lat,
    q_heads, k_heads, v_heads, qu_laid, attended, merged,
    send_sems, recv_sems, back_send, back_recv, local_sems,
):
    me = lax.axis_index("sp")
    dp = lax.axis_index("dp")
    place = {
        "me": me,
        "dp": dp,
        "sp_count": sp_count,
        "dp_count": dp_count,
        "z_count": dp_count // 2,
        "x": me + 1 - 2 * lax.rem(me, 2),
        "y": lax.rem(me + 2, sp_count),
        "far": sp_count - 1 - me,
        "core": dp + 1 - 2 * lax.rem(dp, 2),
    }
    count = tokens.shape[0]
    heads = q_heads.shape[0]
    rank = kvd_all.shape[2]

    barrier = pltpu.get_barrier_semaphore()
    peers = [{"sp": lax.rem(me + step, sp_count)} for step in range(1, sp_count)]
    peers += [{"dp": lax.rem(dp + 2 * step, dp_count)} for step in range(1, dp_count // 2)]
    peers += [{"dp": place["core"]}]
    for peer in peers:
        pl.semaphore_signal(barrier, inc=1, device_id=peer, device_id_type=MESH)
    pl.semaphore_wait(barrier, len(peers))

    copies = Copies(send_sems, recv_sems)
    kvd = WeightGather(copies, place, w_kvdown, kvd_all, None)
    qd = WeightGather(copies, place, w_qdown, qd_all, None)
    kvu = ColumnGather(copies, place, w_kvup, kvu_all, local_sems.at[0])
    qu = ColumnGather(copies, place, w_qup, qu_all, local_sems.at[1])
    wo = WeightGather(copies, place, w_out, wo_all, local_sems.at[2], w_out.shape[0] // 4)
    gathers = (kvd, qd, kvu, qu, wo)
    kvd.start()
    qd.start()
    for gather in gathers:
        gather.keep()

    own_table = table[pl.ds(pl.multiple_of(me * count, SUBLANES), count), :]
    picks = rotary_picks(ROPE, 0, 0)
    rotary = lax.dot_general(
        picks, w_rotary[...], (((0,), (0,)), ((), ())), preferred_element_type=jnp.float32
    ).astype(jnp.bfloat16)
    key_rot = lax.dot_general(
        tokens[...], rotary, (((1,), (1,)), ((), ())), preferred_element_type=jnp.float32
    )
    key_rot = turned(key_rot, own_table)
    lane = lax.broadcasted_iota(jnp.int32, key_rot.shape, 1)
    key_rot = jnp.where(lane < ROPE, key_rot, 0.0).astype(jnp.bfloat16)
    kv_lat[me, :, rank:] = key_rot

    steps = kvd.steps
    for step in steps:
        kvd.spread(step)
        if step > 1:
            kvd.relay(step - 1)
    qu.start()
    kvu.start()
    for step in steps:
        qd.spread(step)
        if step > 1:
            qd.relay(step - 1)
        else:
            kvd.relay(steps[-1])
    wo.start()
    wo.start_tail()
    for step in steps:
        kvd.close(step)
    qd.relay(steps[-1])
    kvd.finish()
    down = kvd_all[...].reshape(-1, rank)
    kv_lat[me, :, :rank] = norm_rows(dot(tokens[...], down), kv_gain[...]).astype(jnp.bfloat16)

    def block_view(buffer, owner, begin, rows):
        return buffer.at[owner, pl.ds(begin, rows), :]

    kv_plane = PlaneSpread(copies, place, functools.partial(block_view, kv_lat), count)
    q_plane = PlaneSpread(copies, place, functools.partial(block_view, q_lat), count)
    kv_plane.send()
    for step in steps:
        qd.close(step)
    qd.finish()
    down = qd_all[...].reshape(-1, qd_all.shape[2])
    q_lat[me] = norm_rows(dot(tokens[...], down), q_gain[...]).astype(jnp.bfloat16)
    q_plane.send()
    kv_plane.relay()

    qu.cross()
    kvu.cross()
    qu.finish()
    laid = qu_all[...].reshape(-1, qu_all.shape[2])
    head_width = NOPE + 2 * ROPE
    for head in range(heads):
        picks = rotary_picks(laid.shape[1], head * (NOPE + ROPE), NOPE)
        qu_laid[:, head * head_width : (head + 1) * head_width] = dot(laid, picks).astype(
            jnp.bfloat16
        )
    q_plane.relay()
    wo.spread(1)
    kvu.finish()
    kv_plane.finish()

    def make_keys(block, _):
        rows = pl.ds(pl.multiple_of(block * count, SUBLANES), count)
        latent = kv_lat[block]
        full = dot(latent[:, :rank], kvu_all[...].reshape(rank, -1)).astype(jnp.bfloat16)
        for head in range(heads):
            at = head * (NOPE + VDIM)
            k_heads[head, rows, :NOPE] = full[:, at : at + NOPE]
            k_heads[head, rows, NOPE:] = latent[:, rank:]
            v_heads[head, rows, :] = full[:, at + NOPE : at + NOPE + VDIM]
        return 0

    lax.fori_loop(0, sp_count, make_keys, 0)
    wo.spread(2)
    q_plane.finish()

    def make_block(block, _):
        rows = pl.ds(pl.multiple_of(block * count, SUBLANES), count)
        full = dot(q_lat[block], qu_laid[...])
        turns = table[rows, :]
        for head in range(heads):
            at = head * head_width
            q_heads[head, rows, :NOPE] = full[:, at : at + NOPE].astype(jnp.bfloat16)
            part = full[:, at + NOPE : at + head_width]
            q_heads[head, rows, NOPE:] = turned(part, turns).astype(jnp.bfloat16)
        return 0

    lax.fori_loop(0, sp_count, make_block, 0)

    chores = [functools.partial(wo.spread, step) for step in steps if step > 2]
    chores += [functools.partial(wo.relay, step) for step in steps]
    chores_now = -(-len(chores) // sp_count)

    factor = (NOPE + ROPE) ** (-0.5) * math.log2(math.e)
    contract = (((1,), (1,)), ((), ()))
    width = heads * VDIM

    def back(block):
        return pltpu.make_async_remote_copy(
            src_ref=attended.at[block],
            dst_ref=merged.at[:, pl.ds(pl.multiple_of(me * width, LANES), width)],
            send_sem=back_send.at[block],
            recv_sem=back_recv.at[me],
            device_id={"sp": block},
            device_id_type=MESH,
        )

    for block in reversed(range(sp_count)):
        begin = block * count

        def one_head(head, _):
            query = q_heads[head, begin : begin + count, :]
            near = lax.dot_general(
                query, k_heads[head, begin : begin + count, :], contract,
                preferred_element_type=jnp.float32,
            )
            row = lax.broadcasted_iota(jnp.int32, near.shape, 0)
            col = lax.broadcasted_iota(jnp.int32, near.shape, 1)
            near = jnp.where(col <= row, near, -jnp.inf)
            top = jnp.max(near, axis=-1, keepdims=True)
            if block:
                far = lax.dot_general(
                    query, k_heads[head, :begin, :], contract, preferred_element_type=jnp.float32
                )
                top = jnp.maximum(top, jnp.max(far, axis=-1, keepdims=True))
            near = jnp.exp2((near - top) * factor)
            total = jnp.sum(near, axis=-1, keepdims=True)
            if block:
                far = jnp.exp2((far - top) * factor)
                total = total + jnp.sum(far, axis=-1, keepdims=True)
            share = 1.0 / total
            result = dot((near * share).astype(jnp.bfloat16), v_heads[head, begin : begin + count, :])
            if block:
                result = result + dot((far * share).astype(jnp.bfloat16), v_heads[head, :begin, :])
            lanes = pl.ds(pl.multiple_of(head * VDIM, LANES), VDIM)
            attended[block, :, lanes] = result.astype(jnp.bfloat16)
            return 0

        lax.fori_loop(0, heads, one_head, 0)

        @pl.when(me != block)
        def _():
            back(block).start()

        @pl.when(me == block)
        def _():
            merged[:, pl.ds(pl.multiple_of(me * width, LANES), width)] = attended[block]

        for chore in chores[:chores_now]:
            chore()
        del chores[:chores_now]

    for step in steps:
        wo.close(step)
    for step in steps:
        wo.cross_tail(step)
    wo.finish()
    for source in range(sp_count):

        @pl.when(me != source)
        def _():
            pltpu.make_async_remote_copy(
                src_ref=attended.at[source],
                dst_ref=merged.at[:, source * width : (source + 1) * width],
                send_sem=back_send.at[source],
                recv_sem=back_recv.at[source],
                device_id={"sp": source},
                device_id_type=MESH,
            ).wait()

    out_width = wo_all.shape[2]

    def project(piece, squares):
        lanes = pl.ds(pl.multiple_of(piece * out_width, LANES), out_width)
        value = dot(merged[...], wo_all[piece])
        out[:, lanes] = value
        return squares + jnp.sum(value * value, axis=-1, keepdims=True)

    squares = lax.fori_loop(0, dp_count, project, jnp.zeros((count, 1), jnp.float32))
    scale = lax.rsqrt(squares * (1.0 / out.shape[1]) + EPSILON)
    out[...] = out[...] * scale * out_gain[...]
    for copy in copies.sent:
        copy.wait_send()


def kernel_body(mesh, tokens, w_qdown, w_kvdown, w_rotary, q_gain, kv_gain, w_qup, w_kvup, w_out, out_gain):
    sp_count, dp_count = mesh.shape["sp"], mesh.shape["dp"]
    heads = HEADS // sp_count
    count, depth = tokens.shape[1:]
    length = count * sp_count
    q_rank, kv_rank = w_qdown.shape[1], w_kvdown.shape[1]
    bf16 = jnp.bfloat16
    steps = dp_count // 2 - 1
    sems = 3 * (9 * steps + 1) + 2 * steps + 2 * (2 * steps + 1) + 2 * 4
    vmem, hbm = pl.BlockSpec(memory_space=pltpu.VMEM), pl.BlockSpec(memory_space=pl.ANY)
    sp_width = HEADS // sp_count
    mixed = pl.pallas_call(
        functools.partial(kernel, sp_count, dp_count),
        out_shape=jax.ShapeDtypeStruct((count, w_out.shape[1] * dp_count), jnp.float32),
        in_specs=[vmem] * 6 + [hbm] * 3 + [vmem] * 2,
        out_specs=vmem,
        scratch_shapes=[
            pltpu.VMEM((dp_count,) + w_qdown.shape, bf16),
            pltpu.VMEM((dp_count,) + w_kvdown.shape, bf16),
            pltpu.VMEM((dp_count, w_qup.shape[0], sp_width * (NOPE + ROPE)), bf16),
            pltpu.VMEM((dp_count, w_kvup.shape[0], sp_width * (NOPE + VDIM)), bf16),
            pltpu.VMEM((dp_count,) + w_out.shape, bf16),
            pltpu.VMEM((sp_count, count, q_rank), bf16),
            pltpu.VMEM((sp_count, count, kv_rank + 2 * ROPE), bf16),
            pltpu.VMEM((heads, length, NOPE + 2 * ROPE), bf16),
            pltpu.VMEM((heads, length, NOPE + 2 * ROPE), bf16),
            pltpu.VMEM((heads, length, VDIM), bf16),
            pltpu.VMEM((q_rank, heads * (NOPE + 2 * ROPE)), bf16),
            pltpu.VMEM((sp_count, count, heads * VDIM), bf16),
            pltpu.VMEM((count, HEADS * VDIM), bf16),
            pltpu.SemaphoreType.DMA((sems,)),
            pltpu.SemaphoreType.DMA((sems,)),
            pltpu.SemaphoreType.DMA((sp_count,)),
            pltpu.SemaphoreType.DMA((sp_count,)),
            pltpu.SemaphoreType.DMA((3,)),
        ],
        compiler_params=pltpu.CompilerParams(
            collective_id=0, has_side_effects=True, vmem_limit_bytes=60 * 1024 * 1024
        ),
        name="latent_attention",
    )(
        tokens[0], w_qdown, w_kvdown, w_rotary.T, q_gain[None], kv_gain[None], w_qup, w_kvup, w_out,
        out_gain[None], jnp.asarray(turn_table(length)),
    )
    return mixed.astype(bf16)[None]


def fits_kernel(mesh):
    return mesh.shape["sp"] == 2 * 2 and mesh.shape["dp"] % 2 == 0


def solution(mesh):
    in_specs = (
        P("dp", "sp", None),
        P("dp", None),
        P("dp", None),
        P(),
        P(),
        P(),
        P("dp", None),
        P("dp", None),
        P(None, "dp"),
        P(),
    )
    out_specs = P("dp", "sp", None)
    body = functools.partial(kernel_body, mesh) if fits_kernel(mesh) else plain_body
    return jax.shard_map(body, mesh=mesh, in_specs=in_specs, out_specs=out_specs, check_vma=False)
```

profile of v0, /device:TPU:29, one launch (start us, length us, event | category | flops | bytes accessed | tf_op | source)
XLA Modules:
  0.0 106.5 jit_solution(7271723423984959597)
XLA Ops:
  0.0 103.8 %latent_attention.1 = f32[256,2048]{1,0:T(8,128)} custom-call(bf16[256,2048]{1,0:T(8,128)(2,1)} %bitcast.7, bf16[256,512]{1,0:T(8,128)(2,1)} %w_qdown.1, bf16[256,512]{1,0:T(8,128)(2,1)} %w_kvdown.1, bf16[64,2048]{1,0:T(8,128)(2,1)} %bitcast.8, f32[1,512]{1,0:T(1,128)} %bitcast.10, f32[1,512]{1,0:T(1,128)} %bitcast.11, bf16[64,3072]{1,0:T(8,128)(2,1)} %w_qup.1, ...), custom_call_target="tpu_custom_call" | custom-call | tf_op jit(solution)/shard_map/latent_attention/pallas_call | solution.py:579
  103.8 2.7 %convert_bitcast_fusion = bf16[1,256,2048]{2,1,0:T(8,128)(2,1)} fusion(f32[256,2048]{1,0:T(8,128)} %latent_attention.1), kind=kLoop, calls=%fused_computation | loop fusion | flops 524288 | bytes 3145728 | tf_op jit(solution)/shard_map/broadcast_in_dim | solution.py:612
where the time goes:
time: 107 us
  Pallas kernels  104 us (97%)
  other arithmetic  2.71 us (3%)
    pallas_call x1, Pallas kernels, kernel_body(): pl.pallas_call(functools.partial(kernel, sp_count, dp_count), out_shape=j...  104 us
    broadcast_in_dim x1, other arithmetic, kernel_body(): return mixed.astype(bf16)[None]  2.71 us

commit v1 on v0

v1 whole, which is shorter than its diff:
```python
import functools
import math

import jax
import jax.numpy as jnp
import numpy as np
from jax import lax
from jax.experimental import pallas as pl
from jax.experimental.pallas import tpu as pltpu
from jax.sharding import PartitionSpec as P

HEADS = 16
NOPE = 128
ROPE = 64
VDIM = 128


EPSILON = 1e-06
THETA = 10000.0
LANES = 128
SUBLANES = 16
MESH = pl.DeviceIdType.MESH


def norm_rows(values, gain):
    scale = lax.rsqrt(jnp.mean(values * values, axis=-1, keepdims=True) + EPSILON)
    return values * scale * gain


def rotate(values, cosine, sine):
    half = values.shape[-1] // 2
    first = values[..., :half]
    second = values[..., half:]
    return jnp.concatenate(
        [first * cosine - second * sine, second * cosine + first * sine], axis=-1
    )


def turn_tables(offset, count):
    positions = (offset + jnp.arange(count)).astype(jnp.float32)
    freqs = THETA ** (-jnp.arange(0, ROPE, 2).astype(jnp.float32) / ROPE)
    angles = positions[:, None] * freqs[None, :]
    return (jnp.cos(angles), jnp.sin(angles))


def make_queries(q_full, cosine, sine, heads_here):
    rows = q_full.shape[0]
    shaped = q_full.reshape(rows, heads_here, NOPE + ROPE)
    turned = rotate(shaped[..., NOPE:], cosine[:, None, :], sine[:, None, :])
    joined = jnp.concatenate([shaped[..., :NOPE], turned], axis=-1)
    return joined.reshape(rows, heads_here * (NOPE + ROPE)).astype(jnp.bfloat16)


def attend(query_heads, keyval_heads, key_rot, heads_here):
    length = query_heads.shape[0]
    block = math.gcd(length, 512)
    scaling = (NOPE + ROPE) ** (-0.5)
    queries = query_heads.reshape(length, heads_here, NOPE + ROPE)
    keyval = keyval_heads.reshape(length, heads_here, NOPE + VDIM)
    keys_all = keyval[..., :NOPE]
    values_all = keyval[..., NOPE:]
    outputs = []
    for begin in range(0, length, block):
        finish = begin + block
        query_block = queries[begin:finish]
        scores = jnp.einsum(
            "qhd,khd->hqk",
            query_block[..., :NOPE],
            keys_all[:finish],
            preferred_element_type=jnp.float32,
        )
        scores = scores + jnp.einsum(
            "qhd,kd->hqk",
            query_block[..., NOPE:],
            key_rot[:finish],
            preferred_element_type=jnp.float32,
        )
        scores = scores * scaling
        query_pos = begin + jnp.arange(block)
        key_pos = jnp.arange(finish)
        allowed = key_pos[None, :] <= query_pos[:, None]
        scores = jnp.where(allowed[None], scores, -jnp.inf)
        top = jnp.max(scores, axis=-1, keepdims=True)
        expo = jnp.exp(scores - top)
        weights = (expo / jnp.sum(expo, axis=-1, keepdims=True)).astype(jnp.bfloat16)
        attended = jnp.einsum(
            "hqk,khd->qhd", weights, values_all[:finish], preferred_element_type=jnp.float32
        )
        outputs.append(attended.astype(jnp.bfloat16))
    return jnp.concatenate(outputs, axis=0).reshape(length, heads_here * VDIM)


def plain_body(tokens, w_qdown, w_kvdown, w_rotary, q_gain, kv_gain, w_qup, w_kvup, w_out, out_gain):
    own_rows = tokens[0]
    tok_count = own_rows.shape[0]
    sp_count = lax.axis_size("sp")
    sp_place = lax.axis_index("sp")
    length = tok_count * sp_count
    heads_here = HEADS // sp_count
    pieces = (
        lax.all_gather(w_qdown, "dp", axis=0, tiled=True),
        lax.all_gather(w_kvdown, "dp", axis=0, tiled=True),
    )
    q_lat = jnp.dot(own_rows, pieces[0], preferred_element_type=jnp.float32)
    kv_lat = jnp.dot(own_rows, pieces[1], preferred_element_type=jnp.float32)
    q_norm = norm_rows(q_lat, q_gain).astype(jnp.bfloat16)
    kv_norm = norm_rows(kv_lat, kv_gain).astype(jnp.bfloat16)
    own_cos, own_sin = turn_tables(sp_place * tok_count, tok_count)
    key_rot = rotate(
        jnp.dot(own_rows, w_rotary, preferred_element_type=jnp.float32), own_cos, own_sin
    ).astype(jnp.bfloat16)
    q_all, kv_all, rot_all = (
        lax.all_gather(q_norm, "sp", axis=0, tiled=True),
        lax.all_gather(kv_norm, "sp", axis=0, tiled=True),
        lax.all_gather(key_rot, "sp", axis=0, tiled=True),
    )
    q_width = heads_here * (NOPE + ROPE)
    kv_width = heads_here * (NOPE + VDIM)
    q_columns = lax.dynamic_slice_in_dim(w_qup, sp_place * q_width, q_width, 1)
    kv_columns = lax.dynamic_slice_in_dim(w_kvup, sp_place * kv_width, kv_width, 1)
    pieces = (
        lax.all_gather(q_columns, "dp", axis=0, tiled=True),
        lax.all_gather(kv_columns, "dp", axis=0, tiled=True),
    )
    q_full = jnp.dot(q_all, pieces[0], preferred_element_type=jnp.float32)
    kv_full = jnp.dot(kv_all, pieces[1], preferred_element_type=jnp.float32)
    all_cos, all_sin = turn_tables(0, length)
    query_heads = make_queries(q_full, all_cos, all_sin, heads_here)
    keyval_heads = kv_full.astype(jnp.bfloat16)
    attended = attend(query_heads, keyval_heads, rot_all, heads_here)
    merged = lax.all_to_all(attended, "sp", split_axis=0, concat_axis=1, tiled=True)
    proj = jnp.dot(
        merged, lax.all_gather(w_out, "dp", axis=1, tiled=True), preferred_element_type=jnp.float32
    )
    mixed = norm_rows(proj, out_gain).astype(jnp.bfloat16)
    return mixed[None]


def turn_table(length):
    positions = np.arange(length, dtype=np.float32)
    freqs = np.float32(THETA) ** (-np.arange(0, ROPE, 2).astype(np.float32) / np.float32(ROPE))
    angles = positions[:, None] * freqs[None, :].astype(np.float32)
    cosine, sine = np.cos(angles), np.sin(angles)
    return np.concatenate([cosine, cosine, sine, sine], axis=1).astype(np.float32)


class Copies:
    def __init__(self, send_sems, recv_sems):
        self.send_sems, self.recv_sems = send_sems, recv_sems
        self.sends = self.receives = 0
        self.sent = []

    def reserve(self, count):
        at = self.receives
        self.receives += count
        assert self.receives <= self.recv_sems.shape[0]
        return at

    def describe(self, source, target, device, send_at, recv_at):
        return pltpu.make_async_remote_copy(
            src_ref=source(),
            dst_ref=target(),
            send_sem=self.send_sems.at[send_at],
            recv_sem=self.recv_sems.at[recv_at],
            device_id=device,
            device_id_type=MESH,
        )

    def start(self, source, target, device, recv_at=None, when=None):
        send_at = self.sends
        self.sends += 1
        assert self.sends <= self.send_sems.shape[0]
        if recv_at is None:
            recv_at = self.reserve(1)

        def make():
            return self.describe(source, target, device, send_at, recv_at)

        guarded(when, lambda: make().start())
        self.sent.append((make, when))
        return lambda: make().wait_recv()

    def drain(self):
        for make, when in self.sent:
            guarded(when, lambda: make().wait_send())


def guarded(when, action):
    if when is None:
        action()
    else:

        @pl.when(when)
        def _():
            action()


class Chain:
    def __init__(self, copies, place, own, view):
        self.copies, self.place, self.own, self.view = copies, place, own, view
        self.arrived = copies.reserve(place["z_count"])

    def start(self):
        place = self.place
        for step in (1, -1):
            near = place["z"] + step
            self.copies.start(
                self.own,
                functools.partial(self.view, place["dp"]),
                {"dp": 2 * near + place["side"]},
                recv_at=self.arrived + place["z"],
                when=place["above"] if step > 0 else place["below"],
            )

    def arrive(self, step):
        place = self.place
        source, slot = place["order"][step], place["slots"][step]
        block = functools.partial(self.view, slot)
        self.copies.describe(
            block, block, {"dp": place["core"]}, 0, self.arrived + source
        ).wait_recv()
        for way in (1, -1):
            onward = place["z"] + way
            coming = source < place["z"] if way > 0 else source > place["z"]
            self.copies.start(
                block,
                block,
                {"dp": 2 * onward + place["side"]},
                recv_at=self.arrived + source,
                when=coming & (place["above"] if way > 0 else place["below"]),
            )


class PlaneSpread:
    def __init__(self, copies, place, view, rows, halves):
        self.copies, self.place, self.view, self.rows = copies, place, view, rows
        self.halves = halves

    def start(self, owner, begin, count, towards):
        block = functools.partial(self.view, self.place[owner], begin, count)
        return self.copies.start(block, block, {"sp": self.place[towards]})

    def send(self):
        rows, half = self.rows, self.rows // 2
        if self.halves:
            self.early_x = self.start("me", 0, half, "x")
            self.early_y = self.start("me", half, half, "y")
            self.late_x = self.start("me", half, half, "x")
            self.late_y = self.start("me", 0, half, "y")
        else:
            self.early_x = self.start("me", 0, rows, "x")
            self.early_y = self.start("me", 0, rows, "y")
            self.late_x = self.late_y = None

    def relay(self):
        half = self.rows // 2
        self.early_x()
        self.first = self.start("x", 0, half, "y")
        self.early_y()
        self.second = self.start("y", half, half, "x")

    def finish_near(self):
        if self.halves:
            self.late_x()
            self.late_y()

    def finish_far(self):
        self.first()
        self.second()


class Gather:
    def __init__(self, copies, place, buffer):
        self.copies, self.place, self.buffer = copies, place, buffer
        self.crossed = []

    def cross(self, source, target):
        self.crossed.append(self.copies.start(source, target, {"dp": self.place["core"]}))

    def finish(self):
        for arrived in self.crossed:
            arrived()


class WeightGather(Gather):
    def __init__(self, copies, place, source, buffer, tail=0, halves=False):
        super().__init__(copies, place, buffer)
        self.source = source
        self.rows = (source.shape[0] - tail) // place["sp_count"]
        self.halves = halves
        self.planes = {}
        start = pl.multiple_of(place["me"] * self.rows, SUBLANES)
        own = lambda: source.at[pl.ds(start, self.rows), :]
        self.chain = Chain(
            copies, place, own, lambda slot: self.piece(slot, place["me"], 0, self.rows)
        )
        if tail:
            rest = pl.ds(source.shape[0] - tail, tail)
            self.tail = lambda slot: buffer.at[slot, rest, :]
            self.tail_chain = Chain(copies, place, lambda: source.at[rest, :], self.tail)

    def piece(self, slot, owner, begin, count):
        start = pl.multiple_of(owner * self.rows + begin, SUBLANES)
        return self.buffer.at[slot, pl.ds(start, count), :]

    def keep(self):
        self.cross(lambda: self.source, lambda: self.buffer.at[self.place["dp"]])

    def cross_piece(self, step, owner):
        slot = self.place["slots"][step]
        block = lambda: self.piece(slot, self.place[owner], 0, self.rows)
        self.cross(block, block)

    def spread(self, step):
        self.chain.arrive(step)
        view = functools.partial(self.piece, self.place["slots"][step])
        plane = PlaneSpread(self.copies, self.place, view, self.rows, self.halves)
        plane.send()
        self.planes[step] = plane
        self.cross_piece(step, "me")

    def relay(self, step):
        self.planes[step].relay()
        if not self.halves:
            self.cross_piece(step, "x")
            self.cross_piece(step, "y")

    def close(self, step):
        self.planes[step].finish_near()
        if self.halves:
            self.cross_piece(step, "x")
            self.cross_piece(step, "y")
        self.planes[step].finish_far()
        self.cross_piece(step, "far")

    def arrive_tail(self, step):
        self.tail_chain.arrive(step)
        slot = self.place["slots"][step]
        block = lambda: self.tail(slot)
        self.cross(block, block)


class ColumnGather(Gather):
    def __init__(self, copies, place, source, buffer):
        super().__init__(copies, place, buffer)
        width = buffer.shape[2]
        start = pl.multiple_of(place["me"] * width, LANES)
        self.own = lambda: source.at[:, pl.ds(start, width)]
        self.view = lambda slot: buffer.at[slot]
        self.chain = Chain(copies, place, self.own, self.view)

    def keep(self):
        self.cross(self.own, lambda: self.buffer.at[self.place["dp"]])

    def arrive(self, step):
        self.chain.arrive(step)
        slot = self.place["slots"][step]
        block = lambda: self.view(slot)
        self.cross(block, block)


def nearest_first(z, z_count, step):
    short = jnp.minimum(z, z_count - 1 - z)
    long_way = jnp.where(2 * z < z_count - 1, 1, -1)
    turn = (step + 1) // 2
    both = z - long_way * turn if step % 2 else z + long_way * turn
    return jnp.where(step <= 2 * short, both, z + long_way * (step - short))


def rotary_picks(rows, offset, skip):
    width = skip + 2 * ROPE
    row = lax.broadcasted_iota(jnp.int32, (rows, width), 0)
    col = lax.broadcasted_iota(jnp.int32, (rows, width), 1)
    half = ROPE // 2
    minus = (col >= skip + ROPE) & (col < skip + ROPE + half)
    origin = jnp.where(
        col < skip + ROPE, col, jnp.where(minus, col - half, col - ROPE - half)
    )
    sign = jnp.where(minus, -1.0, 1.0)
    return jnp.where(row == origin + offset, sign, 0.0).astype(jnp.bfloat16)


def turned(values, table):
    product = values * table
    return product + pltpu.roll(product, ROPE, axis=1)


def dot(left, right):
    return jnp.dot(left, right, preferred_element_type=jnp.float32)


def kernel(
    sp_count, dp_count,
    tokens, w_qdown, w_kvdown, w_rotary, q_gain, kv_gain, w_qup, w_kvup, w_out, out_gain, table,
    out,
    qd_all, kvd_all, qu_all, kvu_all, wo_all, q_lat, kv_lat,
    q_heads, k_heads, v_heads, qu_laid, attended, merged, proj,
    send_sems, recv_sems, back_send, back_recv, local_sems,
):
    scope = jax.named_scope
    me = lax.axis_index("sp")
    dp = lax.axis_index("dp")
    z_count = dp_count // 2
    side = lax.rem(dp, 2)
    z = dp // 2
    steps = range(1, z_count)
    order = {step: nearest_first(z, z_count, step) for step in steps}
    place = {
        "me": me,
        "dp": dp,
        "z": z,
        "side": side,
        "above": z < z_count - 1,
        "below": z > 0,
        "order": order,
        "slots": {step: 2 * order[step] + side for step in steps},
        "sp_count": sp_count,
        "dp_count": dp_count,
        "z_count": z_count,
        "x": me + 1 - 2 * lax.rem(me, 2),
        "y": lax.rem(me + 2, sp_count),
        "far": sp_count - 1 - me,
        "core": dp + 1 - 2 * side,
    }
    count = tokens.shape[0]
    heads = q_heads.shape[0]
    rank = kvd_all.shape[2]

    barrier = pltpu.get_barrier_semaphore()

    def greet(peer):
        pl.semaphore_signal(barrier, inc=1, device_id=peer, device_id_type=MESH)

    for step in range(1, sp_count):
        greet({"sp": lax.rem(me + step, sp_count)})
    greet({"dp": place["core"]})
    guarded(place["above"], lambda: greet({"dp": dp + 2}))
    guarded(place["below"], lambda: greet({"dp": dp - 2}))

    copies = Copies(send_sems, recv_sems)
    kvd = WeightGather(copies, place, w_kvdown, kvd_all)
    qd = WeightGather(copies, place, w_qdown, qd_all)
    kvu = ColumnGather(copies, place, w_kvup, kvu_all)
    qu = ColumnGather(copies, place, w_qup, qu_all)
    wo = WeightGather(copies, place, w_out, wo_all, w_out.shape[0] * 3 // 8, halves=True)
    kept = [
        pltpu.make_async_copy(kvu.own(), kvu_all.at[dp], local_sems.at[0]),
        pltpu.make_async_copy(qu.own(), qu_all.at[dp], local_sems.at[1]),
        pltpu.make_async_copy(w_out, wo_all.at[dp], local_sems.at[2]),
    ]
    for copy in kept:
        copy.start()
    kvd_all[dp] = w_kvdown[...]
    qd_all[dp] = w_qdown[...]

    with scope("barrier"):
        neighbours = place["above"].astype(jnp.int32) + place["below"].astype(jnp.int32)
        pl.semaphore_wait(barrier, sp_count + neighbours)

    kvd.chain.start()
    qd.chain.start()
    for gather in (kvd, qd, kvu, qu, wo):
        gather.keep()

    with scope("keyrot"):
        own_table = table[pl.ds(pl.multiple_of(me * count, SUBLANES), count), :]
        picks = rotary_picks(ROPE, 0, 0)
        rotary = lax.dot_general(
            picks, w_rotary[...], (((0,), (0,)), ((), ())), preferred_element_type=jnp.float32
        ).astype(jnp.bfloat16)
        key_rot = lax.dot_general(
            tokens[...], rotary, (((1,), (1,)), ((), ())), preferred_element_type=jnp.float32
        )
        key_rot = turned(key_rot, own_table)
        lane = lax.broadcasted_iota(jnp.int32, key_rot.shape, 1)
        key_rot = jnp.where(lane < ROPE, key_rot, 0.0).astype(jnp.bfloat16)
        kv_lat[me, :, rank:] = key_rot

    last = steps[-1]
    with scope("kvd_spread"):
        for step in steps:
            kvd.spread(step)
            if step > 1:
                kvd.relay(step - 1)
    kvu.chain.start()
    qu.chain.start()
    with scope("qd_spread"):
        for step in steps:
            qd.spread(step)
            if step > 1:
                qd.relay(step - 1)
            else:
                kvd.relay(last)
    wo.chain.start()
    with scope("kvd_close"):
        for step in steps:
            kvd.close(step)
    with scope("qd_relay"):
        qd.relay(last)
    with scope("kvd_finish"):
        kvd.finish()
    with scope("kv_lat"):
        down = kvd_all[...].reshape(-1, rank)
        kv_lat[me, :, :rank] = norm_rows(dot(tokens[...], down), kv_gain[...]).astype(jnp.bfloat16)

    def block_view(buffer, owner, begin, rows):
        return buffer.at[owner, pl.ds(begin, rows), :]

    kv_plane = PlaneSpread(copies, place, functools.partial(block_view, kv_lat), count, True)
    q_plane = PlaneSpread(copies, place, functools.partial(block_view, q_lat), count, True)
    kv_plane.send()
    with scope("up_arrive"):
        for step in steps[:-1]:
            kvu.arrive(step)
            qu.arrive(step)
    with scope("qd_close"):
        for step in steps:
            qd.close(step)
        qd.finish()
    with scope("q_lat"):
        down = qd_all[...].reshape(-1, qd_all.shape[2])
        q_lat[me] = norm_rows(dot(tokens[...], down), q_gain[...]).astype(jnp.bfloat16)
    with scope("kv_relay"):
        kv_plane.relay()
    q_plane.send()
    with scope("up_last"):
        kvu.arrive(last)
        qu.arrive(last)
    wo.tail_chain.start()
    with scope("wo_spread1"):
        wo.spread(1)
    with scope("q_relay"):
        q_plane.relay()
    with scope("qu_wait"):
        kept[1].wait()
        qu.finish()
    with scope("qu_lay"):
        laid = qu_all[...].reshape(-1, qu_all.shape[2])
        head_width = NOPE + 2 * ROPE
        for head in range(heads):
            picks = rotary_picks(laid.shape[1], head * (NOPE + ROPE), NOPE)
            qu_laid[:, head * head_width : (head + 1) * head_width] = dot(laid, picks).astype(
                jnp.bfloat16
            )
    with scope("wo_relay1"):
        wo.relay(1)
    with scope("kvu_wait"):
        kept[0].wait()
        kvu.finish()
        kv_plane.finish_near()
        kv_plane.finish_far()

    def make_keys(block, _):
        rows = pl.ds(pl.multiple_of(block * count, SUBLANES), count)
        latent = kv_lat[block]
        full = dot(latent[:, :rank], kvu_all[...].reshape(rank, -1)).astype(jnp.bfloat16)
        for head in range(heads):
            at = head * (NOPE + VDIM)
            k_heads[head, rows, :NOPE] = full[:, at : at + NOPE]
            k_heads[head, rows, NOPE:] = latent[:, rank:]
            v_heads[head, rows, :] = full[:, at + NOPE : at + NOPE + VDIM]
        return 0

    with scope("make_keys"):
        lax.fori_loop(0, sp_count, make_keys, 0)
    with scope("wo_spread2"):
        wo.spread(2)
    with scope("q_wait"):
        q_plane.finish_near()
        q_plane.finish_far()

    def make_block(block, _):
        rows = pl.ds(pl.multiple_of(block * count, SUBLANES), count)
        full = dot(q_lat[block], qu_laid[...])
        turns = table[rows, :]
        for head in range(heads):
            at = head * head_width
            q_heads[head, rows, :NOPE] = full[:, at : at + NOPE].astype(jnp.bfloat16)
            part = full[:, at + NOPE : at + head_width]
            q_heads[head, rows, NOPE:] = turned(part, turns).astype(jnp.bfloat16)
        return 0

    with scope("make_q"):
        lax.fori_loop(0, sp_count, make_block, 0)

    factor = (NOPE + ROPE) ** (-0.5) * math.log2(math.e)
    contract = (((1,), (1,)), ((), ()))
    width = heads * VDIM

    def head_lanes(owner, head):
        return pl.ds(pl.multiple_of(owner * width + head * VDIM, LANES), VDIM)

    def back(block, head, source):
        return pltpu.make_async_remote_copy(
            src_ref=attended.at[block, :, head_lanes(0, head)],
            dst_ref=merged.at[:, head_lanes(source, head)],
            send_sem=back_send.at[head, block],
            recv_sem=back_recv.at[head, source],
            device_id={"sp": block},
            device_id_type=MESH,
        )

    def one_head(head, _):
        for block in reversed(range(sp_count)):
            begin = block * count
            query = q_heads[head, begin : begin + count, :]
            near = lax.dot_general(
                query, k_heads[head, begin : begin + count, :], contract,
                preferred_element_type=jnp.float32,
            )
            row = lax.broadcasted_iota(jnp.int32, near.shape, 0)
            col = lax.broadcasted_iota(jnp.int32, near.shape, 1)
            near = jnp.where(col <= row, near, -jnp.inf)
            top = jnp.max(near, axis=-1, keepdims=True)
            if block:
                far = lax.dot_general(
                    query, k_heads[head, :begin, :], contract, preferred_element_type=jnp.float32
                )
                top = jnp.maximum(top, jnp.max(far, axis=-1, keepdims=True))
            near = jnp.exp2((near - top) * factor)
            total = jnp.sum(near, axis=-1, keepdims=True)
            if block:
                far = jnp.exp2((far - top) * factor)
                total = total + jnp.sum(far, axis=-1, keepdims=True)
            share = 1.0 / total
            result = dot((near * share).astype(jnp.bfloat16), v_heads[head, begin : begin + count, :])
            if block:
                result = result + dot((far * share).astype(jnp.bfloat16), v_heads[head, :begin, :])
            attended[block, :, head_lanes(0, head)] = result.astype(jnp.bfloat16)
        for block in range(sp_count):

            @pl.when(me != block)
            def _():
                back(block, head, me).start()

        merged[:, head_lanes(me, head)] = attended[me, :, head_lanes(0, head)]
        return 0

    chores = [[] for _ in range(heads)]
    plan = [functools.partial(wo.spread, step) for step in steps if step > 2]
    plan += [functools.partial(wo.relay, step) for step in steps if step > 1]
    plan += [functools.partial(wo.arrive_tail, step) for step in steps]
    for at, chore in enumerate(plan):
        chores[at * heads // len(plan)].append(chore)
    for head in range(heads):
        with scope("attn"):
            lax.fori_loop(head, head + 1, one_head, 0)
        with scope("chores"):
            for chore in chores[head]:
                chore()

    with scope("wo_wait"):
        for step in steps:
            wo.close(step)
        kept[2].wait()
        wo.finish()
    with scope("a2a_wait"):
        for source in range(sp_count):

            @pl.when(me != source)
            def _():
                for head in range(heads):
                    back(source, head, source).wait()

    out_width = wo_all.shape[2]

    def project(piece, squares):
        lanes = pl.ds(pl.multiple_of(piece * out_width, LANES), out_width)
        value = dot(merged[...], wo_all[piece])
        proj[:, lanes] = value
        return squares + jnp.sum(value * value, axis=-1, keepdims=True)

    with scope("project"):
        squares = lax.fori_loop(0, dp_count, project, jnp.zeros((count, 1), jnp.float32))
        scale = lax.rsqrt(squares * (1.0 / out.shape[1]) + EPSILON)
        out[...] = (proj[...] * scale * out_gain[...]).astype(out.dtype)
    with scope("drain"):
        copies.drain()


def kernel_body(mesh, tokens, w_qdown, w_kvdown, w_rotary, q_gain, kv_gain, w_qup, w_kvup, w_out, out_gain):
    sp_count, dp_count = mesh.shape["sp"], mesh.shape["dp"]
    heads = HEADS // sp_count
    count, depth = tokens.shape[1:]
    length = count * sp_count
    q_rank, kv_rank = w_qdown.shape[1], w_kvdown.shape[1]
    bf16 = jnp.bfloat16
    steps = dp_count // 2 - 1
    sems = 50 * steps + 30
    vmem, hbm = pl.BlockSpec(memory_space=pltpu.VMEM), pl.BlockSpec(memory_space=pl.ANY)
    sp_width = HEADS // sp_count
    mixed = pl.pallas_call(
        functools.partial(kernel, sp_count, dp_count),
        out_shape=jax.ShapeDtypeStruct((count, w_out.shape[1] * dp_count), bf16),
        in_specs=[vmem] * 6 + [hbm] * 3 + [vmem] * 2,
        out_specs=vmem,
        scratch_shapes=[
            pltpu.VMEM((dp_count,) + w_qdown.shape, bf16),
            pltpu.VMEM((dp_count,) + w_kvdown.shape, bf16),
            pltpu.VMEM((dp_count, w_qup.shape[0], sp_width * (NOPE + ROPE)), bf16),
            pltpu.VMEM((dp_count, w_kvup.shape[0], sp_width * (NOPE + VDIM)), bf16),
            pltpu.VMEM((dp_count,) + w_out.shape, bf16),
            pltpu.VMEM((sp_count, count, q_rank), bf16),
            pltpu.VMEM((sp_count, count, kv_rank + 2 * ROPE), bf16),
            pltpu.VMEM((heads, length, NOPE + 2 * ROPE), bf16),
            pltpu.VMEM((heads, length, NOPE + 2 * ROPE), bf16),
            pltpu.VMEM((heads, length, VDIM), bf16),
            pltpu.VMEM((q_rank, heads * (NOPE + 2 * ROPE)), bf16),
            pltpu.VMEM((sp_count, count, heads * VDIM), bf16),
            pltpu.VMEM((count, HEADS * VDIM), bf16),
            pltpu.VMEM((count, w_out.shape[1] * dp_count), jnp.float32),
            pltpu.SemaphoreType.DMA((sems,)),
            pltpu.SemaphoreType.DMA((sems,)),
            pltpu.SemaphoreType.DMA((heads, sp_count)),
            pltpu.SemaphoreType.DMA((heads, sp_count)),
            pltpu.SemaphoreType.DMA((3,)),
        ],
        compiler_params=pltpu.CompilerParams(
            collective_id=0, has_side_effects=True, vmem_limit_bytes=60 * 1024 * 1024
        ),
        name="latent_attention",
    )(
        tokens[0], w_qdown, w_kvdown, w_rotary.T, q_gain[None], kv_gain[None], w_qup, w_kvup, w_out,
        out_gain[None], jnp.asarray(turn_table(length)),
    )
    return mixed[None]


def fits_kernel(mesh):
    return mesh.shape["sp"] == 2 * 2 and mesh.shape["dp"] % 2 == 0


def solution(mesh):
    in_specs = (
        P("dp", "sp", None),
        P("dp", None),
        P("dp", None),
        P(),
        P(),
        P(),
        P("dp", None),
        P("dp", None),
        P(None, "dp"),
        P(),
    )
    out_specs = P("dp", "sp", None)
    body = functools.partial(kernel_body, mesh) if fits_kernel(mesh) else plain_body
    return jax.shard_map(body, mesh=mesh, in_specs=in_specs, out_specs=out_specs, check_vma=False)
```

time: 107 us -> 94.8 us (0.89)
  the two profiles are of different devices: /device:TPU:29 before, /device:TPU:1 now
where the time goes in v1:
time: 94.8 us; the launch traced here: 94.6 us
  Pallas kernels  92.3 us (97%)
  local copies, waits for them, and re-layouts  2.3 us (2%)
    pallas_call x1, Pallas kernels, kernel_body(): pl.pallas_call(functools.partial(kernel, sp_count, dp_count), out_shape=j...  92.3 us
    unnamed x1, local copies, waits for them, and re-layouts  2.3 us

profile of v1, /device:TPU:1, one launch (start us, length us, event | category | flops | bytes accessed | tf_op | source)
XLA Modules:
  0.0 94.6 jit_solution(14714376021289898129)
XLA Ops:
  0.0 92.3 %latent_attention.1 = bf16[256,2048]{1,0:T(8,128)(2,1)} custom-call(bf16[256,2048]{1,0:T(8,128)(2,1)} %bitcast.7, bf16[256,512]{1,0:T(8,128)(2,1)} %w_qdown.1, bf16[256,512]{1,0:T(8,128)(2,1)} %w_kvdown.1, bf16[64,2048]{1,0:T(8,128)(2,1)} %bitcast.8, f32[1,512]{1,0:T(1,128)} %bitcast.10, f32[1,512]{1,0:T(1,128)} %bitcast.11, bf16[64,3072]{1,0:T(8,128)(2,1)} %w_qup.1, ...), custom_call_target="tpu_custom_call" | custom-call | tf_op jit(solution)/shard_map/latent_attention/pallas_call | solution.py:692
  92.3 2.3 %copy.13 = bf16[1,256,2048]{2,1,0:T(8,128)(2,1)} copy(bf16[1,256,2048]{2,1,0:T(8,128)(2,1)} %bitcast.6) | data formatting | bytes 2097152

commit v2 on v1

--- a/solution.py
+++ b/solution.py
@@ -19,6 +19,7 @@
 THETA = 10000.0
 LANES = 128
 SUBLANES = 16
+CHUNKS = 2
 MESH = pl.DeviceIdType.MESH
 
 
@@ -148,41 +149,43 @@
     def __init__(self, send_sems, recv_sems):
         self.send_sems, self.recv_sems = send_sems, recv_sems
         self.sends = self.receives = 0
-        self.sent = []
-
-    def reserve(self, count):
+        self.owed = []
+
+    def reserve(self, count=1):
         at = self.receives
         self.receives += count
         assert self.receives <= self.recv_sems.shape[0]
         return at
 
-    def describe(self, source, target, device, send_at, recv_at):
-        return pltpu.make_async_remote_copy(
-            src_ref=source(),
-            dst_ref=target(),
-            send_sem=self.send_sems.at[send_at],
-            recv_sem=self.recv_sems.at[recv_at],
-            device_id=device,
-            device_id_type=MESH,
-        )
-
-    def start(self, source, target, device, recv_at=None, when=None):
-        send_at = self.sends
+    def reserve_send(self, whole, when=None):
+        at = self.sends
         self.sends += 1
         assert self.sends <= self.send_sems.shape[0]
-        if recv_at is None:
-            recv_at = self.reserve(1)
-
+        self.owed.append((whole, at, when))
+        return at
+
+    def start(self, source, target, device, send_at, recv_at, when=None):
         def make():
-            return self.describe(source, target, device, send_at, recv_at)
+            return pltpu.make_async_remote_copy(
+                src_ref=source(),
+                dst_ref=target(),
+                send_sem=self.send_sems.at[send_at],
+                recv_sem=self.recv_sems.at[recv_at],
+                device_id=device,
+                device_id_type=MESH,
+            )
 
         guarded(when, lambda: make().start())
-        self.sent.append((make, when))
-        return lambda: make().wait_recv()
+
+    def wait(self, whole, at):
+        pltpu.make_async_copy(whole(), whole(), self.recv_sems.at[at]).wait()
 
     def drain(self):
-        for make, when in self.sent:
-            guarded(when, lambda: make().wait_send())
+        for whole, at, when in self.owed:
+            guarded(
+                when,
+                lambda: pltpu.make_async_copy(whole(), whole(), self.send_sems.at[at]).wait(),
+            )
 
 
 def guarded(when, action):
@@ -195,6 +198,31 @@
             action()
 
 
+class Direct:
+    def __init__(self, copies, place, own, view, whole):
+        self.copies, self.place, self.own, self.view = copies, place, own, view
+        self.arrived = copies.reserve(place["z_count"])
+        self.sent = copies.reserve_send(whole)
+
+    def start(self):
+        place = self.place
+        for step in reversed(place["steps"]):
+            self.copies.start(
+                self.own,
+                functools.partial(self.view, place["dp"]),
+                {"dp": place["slots"][step]},
+                self.sent,
+                self.arrived + place["z"],
+            )
+
+    def forward(self, step):
+        pass
+
+    def settle(self, step):
+        source, slot = self.place["order"][step], self.place["slots"][step]
+        self.copies.wait(functools.partial(self.view, slot), self.arrived + source)
+
+
 class Chain:
     def __init__(self, copies, place, own, view):
         self.copies, self.place, self.own, self.view = copies, place, own, view
@@ -202,119 +230,162 @@
 
     def start(self):
         place = self.place
-        for step in (1, -1):
-            near = place["z"] + step
+        block = functools.partial(self.view, place["dp"])
+        for way in (1, -1):
+            onward = place["z"] + way
+            when = place["above"] if way > 0 else place["below"]
             self.copies.start(
                 self.own,
-                functools.partial(self.view, place["dp"]),
-                {"dp": 2 * near + place["side"]},
-                recv_at=self.arrived + place["z"],
-                when=place["above"] if step > 0 else place["below"],
-            )
-
-    def arrive(self, step):
-        place = self.place
-        source, slot = place["order"][step], place["slots"][step]
-        block = functools.partial(self.view, slot)
-        self.copies.describe(
-            block, block, {"dp": place["core"]}, 0, self.arrived + source
-        ).wait_recv()
-        for way in (1, -1):
-            onward = place["z"] + way
-            coming = source < place["z"] if way > 0 else source > place["z"]
-            self.copies.start(
-                block,
                 block,
                 {"dp": 2 * onward + place["side"]},
-                recv_at=self.arrived + source,
-                when=coming & (place["above"] if way > 0 else place["below"]),
+                self.copies.reserve_send(block, when),
+                self.arrived + place["z"],
+                when,
             )
 
+    def passes(self, step):
+        place, source = self.place, self.place["order"][step]
+        rising = (source < place["z"]) & place["above"]
+        sinking = (source > place["z"]) & place["below"]
+        return rising, sinking
+
+    def block(self, step):
+        return functools.partial(self.view, self.place["slots"][step])
+
+    def forward(self, step):
+        place = self.place
+        source, block = place["order"][step], self.block(step)
+        rising, sinking = self.passes(step)
+        sent = self.copies.reserve_send(block, rising | sinking)
+
+        def move():
+            self.copies.wait(block, self.arrived + source)
+            for way in (1, -1):
+                onward = place["z"] + way
+                self.copies.start(
+                    block,
+                    block,
+                    {"dp": 2 * onward + place["side"]},
+                    sent,
+                    self.arrived + source,
+                    rising if way > 0 else sinking,
+                )
+
+        guarded(rising | sinking, move)
+
+    def settle(self, step):
+        source, block = self.place["order"][step], self.block(step)
+        rising, sinking = self.passes(step)
+        guarded(
+            jnp.logical_not(rising | sinking),
+            lambda: self.copies.wait(block, self.arrived + source),
+        )
+
 
 class PlaneSpread:
-    def __init__(self, copies, place, view, rows, halves):
+    def __init__(self, copies, place, view, span, rows, halves, sent):
         self.copies, self.place, self.view, self.rows = copies, place, view, rows
-        self.halves = halves
-
-    def start(self, owner, begin, count, towards):
+        self.span, self.halves, self.sent = span, halves, sent
+        self.early_x, self.early_y, self.rest = (copies.reserve() for _ in range(3))
+
+    def start(self, owner, begin, count, towards, recv_at):
         block = functools.partial(self.view, self.place[owner], begin, count)
-        return self.copies.start(block, block, {"sp": self.place[towards]})
+        self.copies.start(block, block, {"sp": self.place[towards]}, self.sent, recv_at)
 
     def send(self):
         rows, half = self.rows, self.rows // 2
         if self.halves:
-            self.early_x = self.start("me", 0, half, "x")
-            self.early_y = self.start("me", half, half, "y")
-            self.late_x = self.start("me", half, half, "x")
-            self.late_y = self.start("me", 0, half, "y")
+            self.start("me", 0, half, "x", self.early_x)
+            self.start("me", half, half, "y", self.early_y)
+            self.start("me", half, half, "x", self.rest)
+            self.start("me", 0, half, "y", self.rest)
         else:
-            self.early_x = self.start("me", 0, rows, "x")
-            self.early_y = self.start("me", 0, rows, "y")
-            self.late_x = self.late_y = None
+            self.start("me", 0, rows, "x", self.early_x)
+            self.start("me", 0, rows, "y", self.early_y)
 
     def relay(self):
         half = self.rows // 2
-        self.early_x()
-        self.first = self.start("x", 0, half, "y")
-        self.early_y()
-        self.second = self.start("y", half, half, "x")
-
-    def finish_near(self):
-        if self.halves:
-            self.late_x()
-            self.late_y()
-
-    def finish_far(self):
-        self.first()
-        self.second()
+        early = half if self.halves else self.rows
+        self.copies.wait(functools.partial(self.view, self.place["x"], 0, early), self.early_x)
+        self.start("x", 0, half, "y", self.rest)
+        begin = half if self.halves else 0
+        self.copies.wait(functools.partial(self.view, self.place["y"], begin, early), self.early_y)
+        self.start("y", half, half, "x", self.rest)
+
+    def finish(self):
+        self.copies.wait(functools.partial(self.span, 4 if self.halves else 2), self.rest)
 
 
 class Gather:
-    def __init__(self, copies, place, buffer):
+    def __init__(self, copies, place, buffer, groups):
         self.copies, self.place, self.buffer = copies, place, buffer
-        self.crossed = []
-
-    def cross(self, source, target):
-        self.crossed.append(self.copies.start(source, target, {"dp": self.place["core"]}))
+        self.crossed = [copies.reserve() for _ in range(groups)]
+        self.cross_sent = copies.reserve_send(lambda: buffer.at[pl.ds(0, place["z_count"])])
+
+    def cross(self, step, source, target):
+        self.copies.start(
+            source,
+            target,
+            {"dp": self.place["core"]},
+            self.cross_sent,
+            self.crossed[step % len(self.crossed)],
+        )
+
+    def keep(self):
+        self.cross(0, self.own_whole, lambda: self.buffer.at[self.place["dp"]])
 
     def finish(self):
-        for arrived in self.crossed:
-            arrived()
+        self.copies.wait(lambda: self.buffer.at[pl.ds(0, self.place["z_count"])], self.crossed[0])
+
+    def finish_step(self, step):
+        self.copies.wait(lambda: self.buffer.at[0], self.crossed[step])
 
 
 class WeightGather(Gather):
-    def __init__(self, copies, place, source, buffer, tail=0, halves=False):
-        super().__init__(copies, place, buffer)
-        self.source = source
+    def __init__(self, copies, place, source, buffer, tail=0, chunks=1, chained=False):
+        super().__init__(copies, place, buffer, place["z_count"] if chained else 1)
+        self.own_whole = (lambda: source) if chained else (lambda: buffer.at[place["dp"]])
         self.rows = (source.shape[0] - tail) // place["sp_count"]
-        self.halves = halves
+        self.halves = chained
         self.planes = {}
+        self.plane_sent = copies.reserve_send(
+            lambda: buffer.at[pl.ds(0, len(place["steps"])), pl.ds(0, 3 * self.rows), :]
+        )
         start = pl.multiple_of(place["me"] * self.rows, SUBLANES)
         own = lambda: source.at[pl.ds(start, self.rows), :]
-        self.chain = Chain(
-            copies, place, own, lambda slot: self.piece(slot, place["me"], 0, self.rows)
-        )
+        view = lambda slot: self.piece(slot, place["me"], 0, self.rows)
+        if chained:
+            self.chain = Chain(copies, place, own, view)
+        else:
+            whole = lambda: source.at[pl.ds(0, self.rows * len(place["steps"])), :]
+            self.chain = Direct(copies, place, lambda: view(place["dp"]), view, whole)
         if tail:
-            rest = pl.ds(source.shape[0] - tail, tail)
-            self.tail = lambda slot: buffer.at[slot, rest, :]
-            self.tail_chain = Chain(copies, place, lambda: source.at[rest, :], self.tail)
+            part = tail // chunks
+            self.tails = []
+            for at in range(source.shape[0] - tail, source.shape[0], part):
+                rest = pl.ds(at, part)
+                view = lambda slot, rest=rest: buffer.at[slot, rest, :]
+                own = lambda rest=rest: source.at[rest, :]
+                self.tails.append(Chain(copies, place, own, view))
 
     def piece(self, slot, owner, begin, count):
         start = pl.multiple_of(owner * self.rows + begin, SUBLANES)
         return self.buffer.at[slot, pl.ds(start, count), :]
 
-    def keep(self):
-        self.cross(lambda: self.source, lambda: self.buffer.at[self.place["dp"]])
+    def span(self, halves):
+        return self.buffer.at[0, pl.ds(0, halves * (self.rows // 2)), :]
 
     def cross_piece(self, step, owner):
         slot = self.place["slots"][step]
         block = lambda: self.piece(slot, self.place[owner], 0, self.rows)
-        self.cross(block, block)
+        self.cross(step, block, block)
 
     def spread(self, step):
-        self.chain.arrive(step)
+        self.chain.settle(step)
         view = functools.partial(self.piece, self.place["slots"][step])
-        plane = PlaneSpread(self.copies, self.place, view, self.rows, self.halves)
+        plane = PlaneSpread(
+            self.copies, self.place, view, self.span, self.rows, self.halves, self.plane_sent
+        )
         plane.send()
         self.planes[step] = plane
         self.cross_piece(step, "me")
@@ -326,37 +397,38 @@
             self.cross_piece(step, "y")
 
     def close(self, step):
-        self.planes[step].finish_near()
+        self.planes[step].finish()
         if self.halves:
             self.cross_piece(step, "x")
             self.cross_piece(step, "y")
-        self.planes[step].finish_far()
         self.cross_piece(step, "far")
 
-    def arrive_tail(self, step):
-        self.tail_chain.arrive(step)
-        slot = self.place["slots"][step]
-        block = lambda: self.tail(slot)
-        self.cross(block, block)
+    def start_tail(self, chunk):
+        self.tails[chunk].start()
+
+    def forward_tail(self, chunk, step):
+        self.tails[chunk].forward(step)
+
+    def settle_tail(self, chunk, step):
+        tail = self.tails[chunk]
+        tail.settle(step)
+        self.cross(step, tail.block(step), tail.block(step))
 
 
 class ColumnGather(Gather):
     def __init__(self, copies, place, source, buffer):
-        super().__init__(copies, place, buffer)
+        super().__init__(copies, place, buffer, 1)
         width = buffer.shape[2]
         start = pl.multiple_of(place["me"] * width, LANES)
-        self.own = lambda: source.at[:, pl.ds(start, width)]
+        self.own_whole = lambda: source.at[:, pl.ds(start, width)]
         self.view = lambda slot: buffer.at[slot]
-        self.chain = Chain(copies, place, self.own, self.view)
-
-    def keep(self):
-        self.cross(self.own, lambda: self.buffer.at[self.place["dp"]])
-
-    def arrive(self, step):
-        self.chain.arrive(step)
+        self.chain = Chain(copies, place, self.own_whole, self.view)
+
+    def settle(self, step):
+        self.chain.settle(step)
         slot = self.place["slots"][step]
         block = lambda: self.view(slot)
-        self.cross(block, block)
+        self.cross(step, block, block)
 
 
 def nearest_first(z, z_count, step):
@@ -391,9 +463,11 @@
 
 def kernel(
     sp_count, dp_count,
-    tokens, w_qdown, w_kvdown, w_rotary, q_gain, kv_gain, w_qup, w_kvup, w_out, out_gain, table,
+    tokens_in, w_qdown, w_kvdown, rotary_in, q_gain_in, kv_gain_in, w_qup, w_kvup, w_out,
+    out_gain_in, table_in,
     out,
-    qd_all, kvd_all, qu_all, kvu_all, wo_all, q_lat, kv_lat,
+    tokens, w_rotary, q_gain, kv_gain, out_gain, table,
+    qd_all, kvd_all, qu_all, kvu_all, wo_all, q_lat, kv_lat, rot_all,
     q_heads, k_heads, v_heads, qu_laid, attended, merged, proj,
     send_sems, recv_sems, back_send, back_recv, local_sems,
 ):
@@ -417,6 +491,7 @@
         "sp_count": sp_count,
         "dp_count": dp_count,
         "z_count": z_count,
+        "steps": steps,
         "x": me + 1 - 2 * lax.rem(me, 2),
         "y": lax.rem(me + 2, sp_count),
         "far": sp_count - 1 - me,
@@ -434,32 +509,44 @@
     for step in range(1, sp_count):
         greet({"sp": lax.rem(me + step, sp_count)})
     greet({"dp": place["core"]})
-    guarded(place["above"], lambda: greet({"dp": dp + 2}))
-    guarded(place["below"], lambda: greet({"dp": dp - 2}))
+    for step in steps:
+        greet({"dp": lax.rem(dp + 2 * step, dp_count)})
 
     copies = Copies(send_sems, recv_sems)
     kvd = WeightGather(copies, place, w_kvdown, kvd_all)
     qd = WeightGather(copies, place, w_qdown, qd_all)
     kvu = ColumnGather(copies, place, w_kvup, kvu_all)
     qu = ColumnGather(copies, place, w_qup, qu_all)
-    wo = WeightGather(copies, place, w_out, wo_all, w_out.shape[0] * 3 // 8, halves=True)
-    kept = [
-        pltpu.make_async_copy(kvu.own(), kvu_all.at[dp], local_sems.at[0]),
-        pltpu.make_async_copy(qu.own(), qu_all.at[dp], local_sems.at[1]),
-        pltpu.make_async_copy(w_out, wo_all.at[dp], local_sems.at[2]),
+    wo = WeightGather(copies, place, w_out, wo_all, w_out.shape[0] * 7 // 16, chunks=CHUNKS, chained=True)
+    places = [
+        (w_kvdown, kvd_all.at[dp]),
+        (rotary_in, w_rotary),
+        (tokens_in, tokens),
+        (table_in, table),
+        (w_qdown, qd_all.at[dp]),
+        (kv_gain_in, kv_gain),
+        (q_gain_in, q_gain),
+        (out_gain_in, out_gain),
+        (qu.own_whole(), qu_all.at[dp]),
+        (kvu.own_whole(), kvu_all.at[dp]),
+        (w_out, wo_all.at[dp]),
     ]
-    for copy in kept:
-        copy.start()
-    kvd_all[dp] = w_kvdown[...]
-    qd_all[dp] = w_qdown[...]
+    loads = [
+        pltpu.make_async_copy(source, target, local_sems.at[at])
+        for at, (source, target) in enumerate(places)
+    ]
+    for load in loads:
+        load.start()
 
     with scope("barrier"):
-        neighbours = place["above"].astype(jnp.int32) + place["below"].astype(jnp.int32)
-        pl.semaphore_wait(barrier, sp_count + neighbours)
-
+        pl.semaphore_wait(barrier, sp_count + len(steps))
+
+    loads[0].wait()
     kvd.chain.start()
-    qd.chain.start()
-    for gather in (kvd, qd, kvu, qu, wo):
+    kvd.keep()
+    for load in loads[1:8]:
+        load.wait()
+    for gather in (qd, kvu, qu, wo):
         gather.keep()
 
     with scope("keyrot"):
@@ -473,101 +560,58 @@
         )
         key_rot = turned(key_rot, own_table)
         lane = lax.broadcasted_iota(jnp.int32, key_rot.shape, 1)
-        key_rot = jnp.where(lane < ROPE, key_rot, 0.0).astype(jnp.bfloat16)
-        kv_lat[me, :, rank:] = key_rot
+        rot_all[me] = jnp.where(lane < ROPE, key_rot, 0.0).astype(jnp.bfloat16)
 
     last = steps[-1]
-    with scope("kvd_spread"):
-        for step in steps:
-            kvd.spread(step)
-            if step > 1:
-                kvd.relay(step - 1)
-    kvu.chain.start()
-    qu.chain.start()
-    with scope("qd_spread"):
-        for step in steps:
-            qd.spread(step)
-            if step > 1:
-                qd.relay(step - 1)
-            else:
-                kvd.relay(last)
-    wo.chain.start()
-    with scope("kvd_close"):
-        for step in steps:
-            kvd.close(step)
-    with scope("qd_relay"):
-        qd.relay(last)
-    with scope("kvd_finish"):
-        kvd.finish()
-    with scope("kv_lat"):
-        down = kvd_all[...].reshape(-1, rank)
-        kv_lat[me, :, :rank] = norm_rows(dot(tokens[...], down), kv_gain[...]).astype(jnp.bfloat16)
 
     def block_view(buffer, owner, begin, rows):
         return buffer.at[owner, pl.ds(begin, rows), :]
 
-    kv_plane = PlaneSpread(copies, place, functools.partial(block_view, kv_lat), count, True)
-    q_plane = PlaneSpread(copies, place, functools.partial(block_view, q_lat), count, True)
-    kv_plane.send()
-    with scope("up_arrive"):
-        for step in steps[:-1]:
-            kvu.arrive(step)
-            qu.arrive(step)
-    with scope("qd_close"):
-        for step in steps:
-            qd.close(step)
-        qd.finish()
-    with scope("q_lat"):
+    def latent_plane(buffer):
+        sent = copies.reserve_send(lambda: buffer.at[pl.ds(0, 3)])
+        span = lambda halves: buffer.at[pl.ds(0, halves // 2)]
+        view = functools.partial(block_view, buffer)
+        return PlaneSpread(copies, place, view, span, count, True, sent)
+
+    rot_plane = latent_plane(rot_all)
+    kv_plane = latent_plane(kv_lat)
+    q_plane = latent_plane(q_lat)
+
+    def make_kv_latent():
+        down = kvd_all[...].reshape(-1, rank)
+        kv_lat[me] = norm_rows(dot(tokens[...], down), kv_gain[...]).astype(jnp.bfloat16)
+
+    def make_q_latent():
         down = qd_all[...].reshape(-1, qd_all.shape[2])
         q_lat[me] = norm_rows(dot(tokens[...], down), q_gain[...]).astype(jnp.bfloat16)
-    with scope("kv_relay"):
-        kv_plane.relay()
-    q_plane.send()
-    with scope("up_last"):
-        kvu.arrive(last)
-        qu.arrive(last)
-    wo.tail_chain.start()
-    with scope("wo_spread1"):
-        wo.spread(1)
-    with scope("q_relay"):
-        q_plane.relay()
-    with scope("qu_wait"):
-        kept[1].wait()
-        qu.finish()
-    with scope("qu_lay"):
+
+    def lay_queries():
         laid = qu_all[...].reshape(-1, qu_all.shape[2])
-        head_width = NOPE + 2 * ROPE
         for head in range(heads):
             picks = rotary_picks(laid.shape[1], head * (NOPE + ROPE), NOPE)
             qu_laid[:, head * head_width : (head + 1) * head_width] = dot(laid, picks).astype(
                 jnp.bfloat16
             )
-    with scope("wo_relay1"):
-        wo.relay(1)
-    with scope("kvu_wait"):
-        kept[0].wait()
-        kvu.finish()
-        kv_plane.finish_near()
-        kv_plane.finish_far()
+
+    head_width = NOPE + 2 * ROPE
+
+    def do(name, action, *args):
+        with scope(name + "".join(str(a) for a in args)):
+            action(*args)
 
     def make_keys(block, _):
         rows = pl.ds(pl.multiple_of(block * count, SUBLANES), count)
         latent = kv_lat[block]
-        full = dot(latent[:, :rank], kvu_all[...].reshape(rank, -1)).astype(jnp.bfloat16)
+        full = dot(latent, kvu_all[...].reshape(rank, -1)).astype(jnp.bfloat16)
         for head in range(heads):
             at = head * (NOPE + VDIM)
             k_heads[head, rows, :NOPE] = full[:, at : at + NOPE]
-            k_heads[head, rows, NOPE:] = latent[:, rank:]
+            k_heads[head, rows, NOPE:] = rot_all[block]
             v_heads[head, rows, :] = full[:, at + NOPE : at + NOPE + VDIM]
         return 0
 
-    with scope("make_keys"):
+    def make_all_keys():
         lax.fori_loop(0, sp_count, make_keys, 0)
-    with scope("wo_spread2"):
-        wo.spread(2)
-    with scope("q_wait"):
-        q_plane.finish_near()
-        q_plane.finish_far()
 
     def make_block(block, _):
         rows = pl.ds(pl.multiple_of(block * count, SUBLANES), count)
@@ -580,7 +624,7 @@
             q_heads[head, rows, NOPE:] = turned(part, turns).astype(jnp.bfloat16)
         return 0
 
-    with scope("make_q"):
+    def make_all_queries():
         lax.fori_loop(0, sp_count, make_block, 0)
 
     factor = (NOPE + ROPE) ** (-0.5) * math.log2(math.e)
@@ -594,8 +638,8 @@
         return pltpu.make_async_remote_copy(
             src_ref=attended.at[block, :, head_lanes(0, head)],
             dst_ref=merged.at[:, head_lanes(source, head)],
-            send_sem=back_send.at[head, block],
-            recv_sem=back_recv.at[head, source],
+            send_sem=back_send,
+            recv_sem=back_recv,
             device_id={"sp": block},
             device_id_type=MESH,
         )
@@ -636,46 +680,126 @@
         merged[:, head_lanes(me, head)] = attended[me, :, head_lanes(0, head)]
         return 0
 
-    chores = [[] for _ in range(heads)]
-    plan = [functools.partial(wo.spread, step) for step in steps if step > 2]
-    plan += [functools.partial(wo.relay, step) for step in steps if step > 1]
-    plan += [functools.partial(wo.arrive_tail, step) for step in steps]
-    for at, chore in enumerate(plan):
-        chores[at * heads // len(plan)].append(chore)
-    for head in range(heads):
-        with scope("attn"):
-            lax.fori_loop(head, head + 1, one_head, 0)
-        with scope("chores"):
-            for chore in chores[head]:
-                chore()
-
-    with scope("wo_wait"):
-        for step in steps:
-            wo.close(step)
-        kept[2].wait()
-        wo.finish()
-    with scope("a2a_wait"):
-        for source in range(sp_count):
-
-            @pl.when(me != source)
-            def _():
-                for head in range(heads):
-                    back(source, head, source).wait()
-
+    def attend_head(head):
+        lax.fori_loop(head, head + 1, one_head, 0)
+
+    others = attended.at[pl.ds(0, sp_count - 1)]
     out_width = wo_all.shape[2]
 
-    def project(piece, squares):
-        lanes = pl.ds(pl.multiple_of(piece * out_width, LANES), out_width)
-        value = dot(merged[...], wo_all[piece])
-        proj[:, lanes] = value
-        return squares + jnp.sum(value * value, axis=-1, keepdims=True)
-
-    with scope("project"):
-        squares = lax.fori_loop(0, dp_count, project, jnp.zeros((count, 1), jnp.float32))
+    def wait_back():
+        pltpu.make_async_copy(others, others, back_recv).wait()
+
+    def project(step, squares):
+        with scope(f"project{step}"):
+            for core in range(2):
+                piece = 2 * (order[step] if step else z) + core
+                lanes = pl.ds(pl.multiple_of(piece * out_width, LANES), out_width)
+                value = dot(merged[...], wo_all[piece])
+                proj[:, lanes] = value
+                squares = squares + jnp.sum(value * value, axis=-1, keepdims=True)
+        return squares
+
+    rot_plane.send()
+    do("kd_s", kvd.spread, 1)
+    do("kd_s", kvd.spread, 2)
+    qd.chain.start()
+    do("rot_r", rot_plane.relay)
+    do("kd_r", kvd.relay, 1)
+    do("kd_s", kvd.spread, 3)
+    kvu.chain.start()
+    qu.chain.start()
+    wo.chain.start()
+    do("kd_r", kvd.relay, 2)
+    do("kd_r", kvd.relay, 3)
+    do("qd_s", qd.spread, 1)
+    do("qd_s", qd.spread, 2)
+    do("kd_c", kvd.close, 1)
+    do("kd_c", kvd.close, 2)
+    do("qd_r", qd.relay, 1)
+    do("qd_s", qd.spread, 3)
+    do("kd_c", kvd.close, 3)
+    do("kvu_fw", kvu.chain.forward, 1)
+    do("qu_fw", qu.chain.forward, 1)
+    do("kvu_fw", kvu.chain.forward, 2)
+    do("qu_fw", qu.chain.forward, 2)
+    wo.start_tail(0)
+    do("qd_r", qd.relay, 2)
+    do("kd_f", kvd.finish)
+    do("kv_lat", make_kv_latent)
+    kv_plane.send()
+    do("qd_r", qd.relay, 3)
+    do("qd_c", qd.close, 1)
+    do("qd_c", qd.close, 2)
+    do("kv_r", kv_plane.relay)
+    do("qd_c", qd.close, 3)
+    do("qd_f", qd.finish)
+    do("q_lat", make_q_latent)
+    q_plane.send()
+    do("kvu_fw", kvu.chain.forward, 3)
+    do("qu_fw", qu.chain.forward, 3)
+    do("wo_fw", wo.chain.forward, 1)
+    do("wo_fw", wo.chain.forward, 2)
+    do("q_r", q_plane.relay)
+    do("wo_s", wo.spread, 1)
+    do("wo_fw", wo.chain.forward, 3)
+    do("t0_fw", wo.forward_tail, 0, 1)
+    do("t0_fw", wo.forward_tail, 0, 2)
+    wo.start_tail(1)
+    do("qu_st", qu.settle, 1)
+    do("kvu_st", kvu.settle, 1)
+    do("qu_st", qu.settle, 2)
+    do("kvu_st", kvu.settle, 2)
+    do("qu_st", qu.settle, 3)
+    do("kvu_st", kvu.settle, 3)
+    loads[9].wait()
+    do("kvu_f", kvu.finish)
+    do("rot_f", rot_plane.finish)
+    do("kv_f", kv_plane.finish)
+    do("make_keys", make_all_keys)
+    loads[8].wait()
+    do("qu_f", qu.finish)
+    do("qu_lay", lay_queries)
+    do("wo_s", wo.spread, 2)
+    do("wo_r", wo.relay, 1)
+    do("q_f", q_plane.finish)
+    do("make_q", make_all_queries)
+    do("t0_fw", wo.forward_tail, 0, 3)
+    do("attn", attend_head, 0)
+    do("wo_s", wo.spread, 3)
+    do("t1_fw", wo.forward_tail, 1, 1)
+    do("t1_fw", wo.forward_tail, 1, 2)
+    do("attn", attend_head, 1)
+    do("wo_r", wo.relay, 2)
+    do("attn", attend_head, 2)
+    do("t1_fw", wo.forward_tail, 1, 3)
+    do("wo_r", wo.relay, 3)
+    do("attn", attend_head, 3)
+    do("wo_c", wo.close, 1)
+    do("t0_st", wo.settle_tail, 0, 1)
+    do("t0_st", wo.settle_tail, 0, 2)
+    do("t0_st", wo.settle_tail, 0, 3)
+    do("t1_st", wo.settle_tail, 1, 1)
+    do("t1_st", wo.settle_tail, 1, 2)
+    do("wo_c", wo.close, 2)
+    do("t1_st", wo.settle_tail, 1, 3)
+    do("wo_c", wo.close, 3)
+    do("a2a", wait_back)
+    squares = jnp.zeros((count, 1), jnp.float32)
+    loads[10].wait()
+    do("wo_f", wo.finish_step, 0)
+    squares = project(0, squares)
+    do("wo_f", wo.finish_step, 1)
+    squares = project(1, squares)
+    do("wo_f", wo.finish_step, 2)
+    squares = project(2, squares)
+    do("wo_f", wo.finish_step, 3)
+    squares = project(3, squares)
+    with scope("norm"):
         scale = lax.rsqrt(squares * (1.0 / out.shape[1]) + EPSILON)
         out[...] = (proj[...] * scale * out_gain[...]).astype(out.dtype)
     with scope("drain"):
         copies.drain()
+        pltpu.make_async_copy(others, others, back_send).wait()
 
 
 def kernel_body(mesh, tokens, w_qdown, w_kvdown, w_rotary, q_gain, kv_gain, w_qup, w_kvup, w_out, out_gain):
@@ -686,22 +810,31 @@
     q_rank, kv_rank = w_qdown.shape[1], w_kvdown.shape[1]
     bf16 = jnp.bfloat16
     steps = dp_count // 2 - 1
-    sems = 50 * steps + 30
+    chains = 3 + CHUNKS
+    sends = chains * (steps + 2) + 13
+    receives = 3 * 3 * steps + 9 + (chains + 2) * (steps + 1) + 4 + steps + 1
     vmem, hbm = pl.BlockSpec(memory_space=pltpu.VMEM), pl.BlockSpec(memory_space=pl.ANY)
     sp_width = HEADS // sp_count
     mixed = pl.pallas_call(
         functools.partial(kernel, sp_count, dp_count),
-        out_shape=jax.ShapeDtypeStruct((count, w_out.shape[1] * dp_count), bf16),
-        in_specs=[vmem] * 6 + [hbm] * 3 + [vmem] * 2,
+        out_shape=pltpu.VMEM((count, w_out.shape[1] * dp_count), bf16),
+        in_specs=[hbm] * 11,
         out_specs=vmem,
         scratch_shapes=[
+            pltpu.VMEM((count, depth), bf16),
+            pltpu.VMEM(w_rotary.shape[::-1], bf16),
+            pltpu.VMEM((1, q_rank), jnp.float32),
+            pltpu.VMEM((1, kv_rank), jnp.float32),
+            pltpu.VMEM((1, out_gain.shape[0]), jnp.float32),
+            pltpu.VMEM((length, 4 * (ROPE // 2)), jnp.float32),
             pltpu.VMEM((dp_count,) + w_qdown.shape, bf16),
             pltpu.VMEM((dp_count,) + w_kvdown.shape, bf16),
             pltpu.VMEM((dp_count, w_qup.shape[0], sp_width * (NOPE + ROPE)), bf16),
             pltpu.VMEM((dp_count, w_kvup.shape[0], sp_width * (NOPE + VDIM)), bf16),
             pltpu.VMEM((dp_count,) + w_out.shape, bf16),
             pltpu.VMEM((sp_count, count, q_rank), bf16),
-            pltpu.VMEM((sp_count, count, kv_rank + 2 * ROPE), bf16),
+            pltpu.VMEM((sp_count, count, kv_rank), bf16),
+            pltpu.VMEM((sp_count, count, 2 * ROPE), bf16),
             pltpu.VMEM((heads, length, NOPE + 2 * ROPE), bf16),
             pltpu.VMEM((heads, length, NOPE + 2 * ROPE), bf16),
             pltpu.VMEM((heads, length, VDIM), bf16),
@@ -709,11 +842,11 @@
             pltpu.VMEM((sp_count, count, heads * VDIM), bf16),
             pltpu.VMEM((count, HEADS * VDIM), bf16),
             pltpu.VMEM((count, w_out.shape[1] * dp_count), jnp.float32),
-            pltpu.SemaphoreType.DMA((sems,)),
-            pltpu.SemaphoreType.DMA((sems,)),
-            pltpu.SemaphoreType.DMA((heads, sp_count)),
-            pltpu.SemaphoreType.DMA((heads, sp_count)),
-            pltpu.SemaphoreType.DMA((3,)),
+            pltpu.SemaphoreType.DMA((sends,)),
+            pltpu.SemaphoreType.DMA((receives,)),
+            pltpu.SemaphoreType.DMA,
+            pltpu.SemaphoreType.DMA,
+            pltpu.SemaphoreType.DMA((11,)),
         ],
         compiler_params=pltpu.CompilerParams(
             collective_id=0, has_side_effects=True, vmem_limit_bytes=60 * 1024 * 1024

time: 94.8 us -> 78.7 us (0.83)
  Pallas kernels: 92.3 us -> 77.5 us
  local copies, waits for them, and re-layouts: 2.3 us -> 0.97 us
    pallas_call x1, Pallas kernels: 92.3 us -> 77.5 us  [kernel_body(): pl.pallas_call(functools.partial(kernel, sp_count, dp_count), out_shape=p...]
    unnamed x1, local copies, waits for them, and re-layouts: 2.3 us -> 0.97 us
where the time goes in v2:
time: 78.7 us; the launch traced here: 78.5 us
  Pallas kernels  77.5 us (98%)
  local copies, waits for them, and re-layouts  0.97 us (1%)
    pallas_call x1, Pallas kernels, kernel_body(): pl.pallas_call(functools.partial(kernel, sp_count, dp_count), out_shape=p...  77.5 us

profile of v2, /device:TPU:1, one launch (start us, length us, event | category | flops | bytes accessed | tf_op | source)
XLA Modules:
  0.0 78.5 jit_solution(17043664603069929989)
XLA Ops:
  0.0 77.5 %latent_attention.1 = bf16[256,2048]{1,0:T(8,128)(2,1)S(1)} custom-call(bf16[256,2048]{1,0:T(8,128)(2,1)} %bitcast.7, bf16[256,512]{1,0:T(8,128)(2,1)} %w_qdown.1, bf16[256,512]{1,0:T(8,128)(2,1)} %w_kvdown.1, bf16[64,2048]{1,0:T(8,128)(2,1)} %bitcast.8, f32[1,512]{1,0:T(1,128)} %bitcast.10, f32[1,512]{1,0:T(1,128)} %bitcast.11, bf16[64,3072]{1,0:T(8,128)(2,1)} %w_qup.1, ...), custom_call_target="tpu_custom_call" | custom-call | tf_op jit(solution)/shard_map/latent_attention/pallas_call | solution.py:818
  77.5 1.0 %copy.13 = bf16[1,256,2048]{2,1,0:T(8,128)(2,1)} copy(bf16[1,256,2048]{2,1,0:T(8,128)(2,1)S(1)} %bitcast.6) | data formatting | bytes 2097152

commit v3 on v2

--- a/solution.py
+++ b/solution.py
@@ -712,12 +712,12 @@
     do("kd_r", kvd.relay, 2)
     do("kd_r", kvd.relay, 3)
     do("qd_s", qd.spread, 1)
+    do("kd_c", kvd.close, 1)
     do("qd_s", qd.spread, 2)
-    do("kd_c", kvd.close, 1)
+    do("qd_s", qd.spread, 3)
     do("kd_c", kvd.close, 2)
+    do("kd_c", kvd.close, 3)
     do("qd_r", qd.relay, 1)
-    do("qd_s", qd.spread, 3)
-    do("kd_c", kvd.close, 3)
     do("kvu_fw", kvu.chain.forward, 1)
     do("qu_fw", qu.chain.forward, 1)
     do("kvu_fw", kvu.chain.forward, 2)
@@ -726,8 +726,10 @@
     do("qd_r", qd.relay, 2)
     do("kd_f", kvd.finish)
     do("kv_lat", make_kv_latent)
+    do("qd_r", qd.relay, 3)
     kv_plane.send()
-    do("qd_r", qd.relay, 3)
+    do("kvu_fw", kvu.chain.forward, 3)
+    do("qu_fw", qu.chain.forward, 3)
     do("qd_c", qd.close, 1)
     do("qd_c", qd.close, 2)
     do("kv_r", kv_plane.relay)
@@ -735,8 +737,6 @@
     do("qd_f", qd.finish)
     do("q_lat", make_q_latent)
     q_plane.send()
-    do("kvu_fw", kvu.chain.forward, 3)
-    do("qu_fw", qu.chain.forward, 3)
     do("wo_fw", wo.chain.forward, 1)
     do("wo_fw", wo.chain.forward, 2)
     do("q_r", q_plane.relay)
@@ -779,10 +779,8 @@
     do("t0_st", wo.settle_tail, 0, 2)
     do("t0_st", wo.settle_tail, 0, 3)
     do("t1_st", wo.settle_tail, 1, 1)
+    do("wo_c", wo.close, 2)
     do("t1_st", wo.settle_tail, 1, 2)
-    do("wo_c", wo.close, 2)
-    do("t1_st", wo.settle_tail, 1, 3)
-    do("wo_c", wo.close, 3)
     do("a2a", wait_back)
     squares = jnp.zeros((count, 1), jnp.float32)
     loads[10].wait()
@@ -790,6 +788,8 @@
     squares = project(0, squares)
     do("wo_f", wo.finish_step, 1)
     squares = project(1, squares)
+    do("wo_c", wo.close, 3)
+    do("t1_st", wo.settle_tail, 1, 3)
     do("wo_f", wo.finish_step, 2)
     squares = project(2, squares)
     do("wo_f", wo.finish_step, 3)

time: 78.7 us -> 76 us (0.966)
  Pallas kernels: 77.5 us -> 74.9 us
    pallas_call x1, Pallas kernels: 77.5 us -> 74.9 us  [kernel_body(): pl.pallas_call(functools.partial(kernel, sp_count, dp_count), out_shape=p...]
where the time goes in v3:
time: 76 us; the launch traced here: 75.8 us
  Pallas kernels  74.9 us (99%)
  local copies, waits for them, and re-layouts  0.97 us (1%)
    pallas_call x1, Pallas kernels, kernel_body(): pl.pallas_call(functools.partial(kernel, sp_count, dp_count), out_shape=p...  74.9 us

profile of v3, /device:TPU:1, one launch (start us, length us, event | category | flops | bytes accessed | tf_op | source)
XLA Modules:
  0.0 75.8 jit_solution(10076262654438638380)
XLA Ops:
  0.0 74.9 %latent_attention.1 = bf16[256,2048]{1,0:T(8,128)(2,1)S(1)} custom-call(bf16[256,2048]{1,0:T(8,128)(2,1)} %bitcast.7, bf16[256,512]{1,0:T(8,128)(2,1)} %w_qdown.1, bf16[256,512]{1,0:T(8,128)(2,1)} %w_kvdown.1, bf16[64,2048]{1,0:T(8,128)(2,1)} %bitcast.8, f32[1,512]{1,0:T(1,128)} %bitcast.10, f32[1,512]{1,0:T(1,128)} %bitcast.11, bf16[64,3072]{1,0:T(8,128)(2,1)} %w_qup.1, ...), custom_call_target="tpu_custom_call" | custom-call | tf_op jit(solution)/shard_map/latent_attention/pallas_call | solution.py:818
  74.9 1.0 %copy.13 = bf16[1,256,2048]{2,1,0:T(8,128)(2,1)} copy(bf16[1,256,2048]{2,1,0:T(8,128)(2,1)S(1)} %bitcast.6) | data formatting | bytes 2097152

commit v4 on v3

--- a/solution.py
+++ b/solution.py
@@ -634,12 +634,15 @@
     def head_lanes(owner, head):
         return pl.ds(pl.multiple_of(owner * width + head * VDIM, LANES), VDIM)
 
+    def merged_lanes(source, head):
+        return pl.ds(pl.multiple_of(head * (sp_count * VDIM) + source * VDIM, LANES), VDIM)
+
     def back(block, head, source):
         return pltpu.make_async_remote_copy(
             src_ref=attended.at[block, :, head_lanes(0, head)],
-            dst_ref=merged.at[:, head_lanes(source, head)],
+            dst_ref=merged.at[:, merged_lanes(source, head)],
             send_sem=back_send,
-            recv_sem=back_recv,
+            recv_sem=back_recv.at[head],
             device_id={"sp": block},
             device_id_type=MESH,
         )
@@ -677,7 +680,7 @@
             def _():
                 back(block, head, me).start()
 
-        merged[:, head_lanes(me, head)] = attended[me, :, head_lanes(0, head)]
+        merged[:, merged_lanes(me, head)] = attended[me, :, head_lanes(0, head)]
         return 0
 
     def attend_head(head):
@@ -686,16 +689,27 @@
     others = attended.at[pl.ds(0, sp_count - 1)]
     out_width = wo_all.shape[2]
 
-    def wait_back():
-        pltpu.make_async_copy(others, others, back_recv).wait()
-
-    def project(step, squares):
-        with scope(f"project{step}"):
-            for core in range(2):
-                piece = 2 * (order[step] if step else z) + core
-                lanes = pl.ds(pl.multiple_of(piece * out_width, LANES), out_width)
-                value = dot(merged[...], wo_all[piece])
-                proj[:, lanes] = value
+    def wait_back(begin, finish):
+        for head in range(begin, finish):
+            part = attended.at[pl.ds(0, sp_count - 1), :, head_lanes(0, head)]
+            pltpu.make_async_copy(part, part, back_recv.at[head]).wait()
+
+    def project(step, begin, finish):
+        squares = jnp.zeros((count, 1), jnp.float32)
+        for core in range(2):
+            piece = 2 * (order[step] if step else z) + core
+            lanes = pl.ds(pl.multiple_of(piece * out_width, LANES), out_width)
+            rows = [
+                wo_all[piece, pl.ds(source * width + head * VDIM, VDIM), :]
+                for head in range(begin, finish)
+                for source in range(sp_count)
+            ]
+            whole = sp_count * VDIM
+            value = dot(merged[:, begin * whole : finish * whole], jnp.concatenate(rows, axis=0))
+            if begin:
+                value = value + proj[:, lanes]
+            proj[:, lanes] = value
+            if finish == heads:
                 squares = squares + jnp.sum(value * value, axis=-1, keepdims=True)
         return squares
 
@@ -781,19 +795,30 @@
     do("t1_st", wo.settle_tail, 1, 1)
     do("wo_c", wo.close, 2)
     do("t1_st", wo.settle_tail, 1, 2)
-    do("a2a", wait_back)
+    do("a2a", wait_back, 0, 3)
     squares = jnp.zeros((count, 1), jnp.float32)
     loads[10].wait()
     do("wo_f", wo.finish_step, 0)
-    squares = project(0, squares)
+    with scope("project00"):
+        project(0, 0, 3)
     do("wo_f", wo.finish_step, 1)
-    squares = project(1, squares)
+    with scope("project10"):
+        project(1, 0, 3)
+    do("wo_f", wo.finish_step, 2)
+    with scope("project20"):
+        project(2, 0, 3)
     do("wo_c", wo.close, 3)
+    do("a2a", wait_back, 3, 4)
+    with scope("project03"):
+        squares = squares + project(0, 3, 4)
+    with scope("project13"):
+        squares = squares + project(1, 3, 4)
+    with scope("project23"):
+        squares = squares + project(2, 3, 4)
     do("t1_st", wo.settle_tail, 1, 3)
-    do("wo_f", wo.finish_step, 2)
-    squares = project(2, squares)
     do("wo_f", wo.finish_step, 3)
-    squares = project(3, squares)
+    with scope("project30"):
+        squares = squares + project(3, 0, 4)
     with scope("norm"):
         scale = lax.rsqrt(squares * (1.0 / out.shape[1]) + EPSILON)
         out[...] = (proj[...] * scale * out_gain[...]).astype(out.dtype)
@@ -845,7 +870,7 @@
             pltpu.SemaphoreType.DMA((sends,)),
             pltpu.SemaphoreType.DMA((receives,)),
             pltpu.SemaphoreType.DMA,
-            pltpu.SemaphoreType.DMA,
+            pltpu.SemaphoreType.DMA((heads,)),
             pltpu.SemaphoreType.DMA((11,)),
         ],
         compiler_params=pltpu.CompilerParams(

time: 76 us -> 75.1 us (0.988)
  Pallas kernels: 74.9 us -> 74 us
    pallas_call x1, Pallas kernels: 74.9 us -> 74 us  [kernel_body(): pl.pallas_call(functools.partial(kernel, sp_count, dp_count), out_shape=p...]
where the time goes in v4:
time: 75.1 us; the launch traced here: 75 us
  Pallas kernels  74 us (99%)
  local copies, waits for them, and re-layouts  0.97 us (1%)
    pallas_call x1, Pallas kernels, kernel_body(): pl.pallas_call(functools.partial(kernel, sp_count, dp_count), out_shape=p...  74 us

profile of v4, /device:TPU:1, one launch (start us, length us, event | category | flops | bytes accessed | tf_op | source)
XLA Modules:
  0.0 75.0 jit_solution(8876804480417959963)
XLA Ops:
  0.0 74.0 %latent_attention.1 = bf16[256,2048]{1,0:T(8,128)(2,1)S(1)} custom-call(bf16[256,2048]{1,0:T(8,128)(2,1)} %bitcast.7, bf16[256,512]{1,0:T(8,128)(2,1)} %w_qdown.1, bf16[256,512]{1,0:T(8,128)(2,1)} %w_kvdown.1, bf16[64,2048]{1,0:T(8,128)(2,1)} %bitcast.8, f32[1,512]{1,0:T(1,128)} %bitcast.10, f32[1,512]{1,0:T(1,128)} %bitcast.11, bf16[64,3072]{1,0:T(8,128)(2,1)} %w_qup.1, ...), custom_call_target="tpu_custom_call" | custom-call | tf_op jit(solution)/shard_map/latent_attention/pallas_call | solution.py:843
  74.0 1.0 %copy.13 = bf16[1,256,2048]{2,1,0:T(8,128)(2,1)} copy(bf16[1,256,2048]{2,1,0:T(8,128)(2,1)S(1)} %bitcast.6) | data formatting | bytes 2097152

commit v5 on v4

--- a/solution.py
+++ b/solution.py
@@ -342,11 +342,11 @@
 
 
 class WeightGather(Gather):
-    def __init__(self, copies, place, source, buffer, tail=0, chunks=1, chained=False):
+    def __init__(self, copies, place, source, buffer, tail=0, chunks=1, chained=False, halves=True):
         super().__init__(copies, place, buffer, place["z_count"] if chained else 1)
         self.own_whole = (lambda: source) if chained else (lambda: buffer.at[place["dp"]])
         self.rows = (source.shape[0] - tail) // place["sp_count"]
-        self.halves = chained
+        self.halves = halves
         self.planes = {}
         self.plane_sent = copies.reserve_send(
             lambda: buffer.at[pl.ds(0, len(place["steps"])), pl.ds(0, 3 * self.rows), :]
@@ -716,10 +716,10 @@
     rot_plane.send()
     do("kd_s", kvd.spread, 1)
     do("kd_s", kvd.spread, 2)
+    do("rot_r", rot_plane.relay)
     qd.chain.start()
-    do("rot_r", rot_plane.relay)
+    do("kd_s", kvd.spread, 3)
     do("kd_r", kvd.relay, 1)
-    do("kd_s", kvd.spread, 3)
     kvu.chain.start()
     qu.chain.start()
     wo.chain.start()
@@ -774,10 +774,10 @@
     do("qu_f", qu.finish)
     do("qu_lay", lay_queries)
     do("wo_s", wo.spread, 2)
-    do("wo_r", wo.relay, 1)
     do("q_f", q_plane.finish)
     do("make_q", make_all_queries)
     do("t0_fw", wo.forward_tail, 0, 3)
+    do("wo_r", wo.relay, 1)
     do("attn", attend_head, 0)
     do("wo_s", wo.spread, 3)
     do("t1_fw", wo.forward_tail, 1, 1)

time: 75.1 us -> 74.8 us (level)
  no operation moved by 1% of the time
where the time goes in v5:
time: 74.8 us; the launch traced here: 74.6 us
  Pallas kernels  73.7 us (99%)
  local copies, waits for them, and re-layouts  0.97 us (1%)
    pallas_call x1, Pallas kernels, kernel_body(): pl.pallas_call(functools.partial(kernel, sp_count, dp_count), out_shape=p...  73.7 us

profile of v5, /device:TPU:1, one launch (start us, length us, event | category | flops | bytes accessed | tf_op | source)
XLA Modules:
  0.0 74.6 jit_solution(15728829238708146721)
XLA Ops:
  0.0 73.7 %latent_attention.1 = bf16[256,2048]{1,0:T(8,128)(2,1)S(1)} custom-call(bf16[256,2048]{1,0:T(8,128)(2,1)} %bitcast.7, bf16[256,512]{1,0:T(8,128)(2,1)} %w_qdown.1, bf16[256,512]{1,0:T(8,128)(2,1)} %w_kvdown.1, bf16[64,2048]{1,0:T(8,128)(2,1)} %bitcast.8, f32[1,512]{1,0:T(1,128)} %bitcast.10, f32[1,512]{1,0:T(1,128)} %bitcast.11, bf16[64,3072]{1,0:T(8,128)(2,1)} %w_qup.1, ...), custom_call_target="tpu_custom_call" | custom-call | tf_op jit(solution)/shard_map/latent_attention/pallas_call | solution.py:843
  73.7 1.0 %copy.13 = bf16[1,256,2048]{2,1,0:T(8,128)(2,1)} copy(bf16[1,256,2048]{2,1,0:T(8,128)(2,1)S(1)} %bitcast.6) | data formatting | bytes 2097152
